TPU v7x, 32 devices: a whole 2x2x4 slice. The times are simulated.
32 devices in a mesh: rep: 2 (over y), fs: 4 (over z), tp: 4 (over x, core).
Axes of the slice: x: 2, y: 2, z: 4, core: 2. Of those that a mesh axis runs over, the one named last changes fastest.
Arguments:
- tokens: bfloat16 [2048, 2048], P(('rep', 'fs')), may hold values from -6 to 6
- mix_gain: float32 [2048], replicated, may hold values from 0.1 to 1.9
- group_weight: float32 [512, 2048], P('fs', 'tp'), may hold values from -0.25 to 0.25
- group_scale: float32 [1, 2048], P(None, 'tp'), may hold values from 0.5 to 2
- mlp_gain: float32 [2048], replicated, may hold values from 0.1 to 1.9
- up_weight: float32 [2048, 8192], P('fs', 'tp'), may hold values from -0.125 to 0.125
- up_scale: float32 [1, 8192], P(None, 'tp'), may hold values from 0.5 to 2
- down_weight: float32 [8192, 2048], P('tp', 'fs'), may hold values from -0.0625 to 0.0625
- down_scale: float32 [1, 2048], replicated, may hold values from 0.5 to 2
Outputs:
- layer_out: bfloat16 [2048, 2048], P(('rep', 'fs'))
All inputs are finite; a program needn't handle non-finite values.
Results may differ from a plain program's by a relative error of at most 0.013.
Values may be sent and summed in bfloat16 or wider, within the bound.
No kernel may reach another device: no remote copies, remote signals or barrier semaphores. Data moves between devices by JAX's collectives and lax.ppermute only.
A program may use at most 64 MiB of HBM per device.

v0:
```python
import jax
import jax.numpy as jnp
from jax import lax
from jax.sharding import PartitionSpec as P

GROUPS = 4
LENGTH = 128


norm_eps = 1e-06


def norm_rows(values, gain):
    promoted = values.astype(jnp.float32)
    inverse = lax.rsqrt(jnp.mean(promoted * promoted, axis=-1, keepdims=True) + norm_eps)
    return (promoted * inverse * gain).astype(jnp.bfloat16)


def band_means(inputs, window, seq_length):
    row_count, columns = inputs.shape
    by_sequence = inputs.reshape(row_count // seq_length, seq_length, columns)
    position = jnp.arange(seq_length, dtype=jnp.int32)
    offset = position[:, None] - position[None, :]
    band_mask = ((offset >= 0) & (offset < window)).astype(jnp.bfloat16)
    divisor = jnp.minimum(position + 1, window).astype(jnp.float32)
    summed = jnp.einsum("ts,nsc->ntc", band_mask, by_sequence, preferred_element_type=jnp.float32)
    return (summed / divisor[None, :, None] - by_sequence.astype(jnp.float32)).reshape(
        row_count, columns
    )


def body(
    tokens,
    mix_gain,
    group_weight,
    group_scale,
    mlp_gain,
    up_weight,
    up_scale,
    down_weight,
    down_scale,
):
    model_width = tokens.shape[1]
    group_width = model_width // GROUPS
    own_cols = group_weight.shape[1]
    column_start = lax.axis_index("tp") * own_cols
    group_index = column_start // group_width
    normed = norm_rows(tokens, mix_gain)
    inputs = lax.dynamic_slice_in_dim(normed, group_index * group_width, group_width, 1)
    window = jnp.left_shift(jnp.int32(2), group_index)
    pooled = band_means(inputs, window, LENGTH).astype(jnp.bfloat16)
    mixed_cols = (
        jnp.dot(
            pooled,
            lax.all_gather(group_weight.astype(jnp.bfloat16), "fs", axis=0, tiled=True),
            preferred_element_type=jnp.float32,
        )
        * group_scale
    )
    own_tokens = lax.dynamic_slice_in_dim(tokens, column_start, own_cols, 1)
    carried_cols = (own_tokens.astype(jnp.float32) + mixed_cols).astype(jnp.bfloat16)
    carried = lax.all_gather(carried_cols, "tp", axis=1, tiled=True)
    normed_mlp = norm_rows(carried, mlp_gain)
    pre_act = (
        jnp.dot(
            normed_mlp,
            lax.all_gather(up_weight.astype(jnp.bfloat16), "fs", axis=0, tiled=True),
            preferred_element_type=jnp.float32,
        )
        * up_scale
    )
    hidden = jnp.square(jax.nn.relu(pre_act)).astype(jnp.bfloat16)
    partial_value = (
        jnp.dot(
            hidden,
            lax.all_gather(down_weight.astype(jnp.bfloat16), "fs", axis=1, tiled=True),
            preferred_element_type=jnp.float32,
        )
        * down_scale
    )
    summed = lax.psum(partial_value.astype(jnp.bfloat16), "tp").astype(jnp.float32)
    return (carried.astype(jnp.float32) + summed).astype(jnp.bfloat16)


def solution(mesh):
    in_specs = (
        P(("rep", "fs"), None),
        P(),
        P("fs", "tp"),
        P(None, "tp"),
        P(),
        P("fs", "tp"),
        P(None, "tp"),
        P("tp", "fs"),
        P(),
    )
    out_specs = P(("rep", "fs"), None)
    return jax.shard_map(body, mesh=mesh, in_specs=in_specs, out_specs=out_specs, check_vma=False)
```

profile of v0, /device:TPU:0, one launch (start us, length us, event | category | flops | bytes accessed | tf_op | source)
XLA Modules:
  0.0 404.8 jit_solution(14775882686962388429)
XLA Ops:
  6.5 0.0 all-gather.4.cloned.1.call-start
  6.5 0.0 copy-start.1
  6.5 1.6 multiply_reduce_fusion
  8.1 1.5 convert_element_type.58
  9.6 0.0 copy-start.2
  9.6 0.0 copy-done.1
  9.6 17.4 %all_gather.12 = bf16[512,512]{1,0:T(8,128)(2,1)S(1)} all-gather(bf16[128,512]{1,0:T(8,128)(2,1)S(1)} %convert_element_type.64), channel_id=1, replica_groups=mesh['rep'=2,'fs'=4,'tp'=4] {'fs'}, dimensions={0}, use_global_device_ids=true | all-gather | bytes 655360 | tf_op jit(solution)/shard_map/all_gather | solution.py:55
  27.0 0.8 dynamic-slice
  27.8 0.1 fusion.19
  27.9 0.2 fusion.12
  28.1 0.0 copy-done.2
  28.1 2.0 fusion.11
  30.1 0.0 all-gather.4.cloned.1.call-update
  30.1 0.0 all-gather.6.cloned.1.call-start
  30.2 3.8 convert_element_type.68
  34.0 0.0 all-gather.6.cloned.1.call-update
  34.0 0.0 all-gather.8.cloned.1.call-start
  34.1 3.8 convert_element_type.70
  37.9 0.0 copy-start.3
  37.9 0.0 copy-start.4
  37.9 0.0 copy-start.5
  37.9 0.0 all-gather.8.cloned.1.call-update
  37.9 0.0 all-reduce.2.cloned.1.call-start
  37.9 10.8 %all-gather.4.cloned.1.call-done = bf16[256,2048]{1,0:T(8,128)(2,1)} async-done(((bf16[256,512]{1,0:T(8,128)(2,1)}), bf16[256,2048]{1,0:T(8,128)(2,1)}) %all-gather.4.cloned.1.call-update) | async-done | bytes 1048592 | tf_op jit(solution)/shard_map/all_gather | solution.py:62
  48.7 1.5 fusion.4
  50.2 149.7 %all-gather.6.cloned.1.call-done = bf16[2048,2048]{1,0:T(8,128)(2,1)} async-done(((bf16[512,2048]{1,0:T(8,128)(2,1)}), bf16[2048,2048]{1,0:T(8,128)(2,1)}) %all-gather.6.cloned.1.call-update) | async-done | bytes 8388624 | tf_op jit(solution)/shard_map/all_gather | solution.py:67
  199.9 149.4 %all-gather.8.cloned.1.call-done = bf16[2048,2048]{1,0:T(8,128)(2,1)} async-done(((bf16[2048,512]{1,0:T(8,128)(2,1)}), bf16[2048,2048]{1,0:T(8,128)(2,1)}) %all-gather.8.cloned.1.call-update) | async-done | bytes 8388624 | tf_op jit(solution)/shard_map/all_gather | solution.py:76
  349.3 0.0 copy-done.3
  349.3 0.0 copy-done.4
  349.3 0.0 copy-done.5
  349.3 0.0 copy-start
  349.4 11.7 %fusion.2 = bf16[256,2048]{1,0:T(8,128)(2,1)} fusion(bf16[2048,2048]{1,0:T(8,128)(2,1)} %all-gather.8.cloned.1.call-done, f32[2048]{0:T(1024)S(1)} %bitcast.22, bf16[2048,2048]{1,0:T(8,128)(2,1)} %all-gather.6.cloned.1.call-done, bf16[256,2048]{1,0:T(8,128)(2,1)} %all-gather.4.cloned.1.call-done, f32[2048]{0:T(1024)S(1)} %bitcast.23, ...), kind=kOutput, calls=%fused_computation.7 | convolution fusion | flops 4300210176 | bytes 18899968 | tf_op jit(solution)/shard_map/dot_general | solution.py:74
  361.1 0.0 all-reduce.2.cloned.1.call-update
  361.1 34.6 %all-reduce.2.cloned.1.call-done = bf16[256,2048]{1,0:T(8,128)(2,1)} async-done(((bf16[256,2048]{1,0:T(8,128)(2,1)}), bf16[256,2048]{1,0:T(8,128)(2,1)}) %all-reduce.2.cloned.1.call-update) | async-done | bytes 1048592 | tf_op jit(solution)/shard_map/psum | solution.py:81
  395.7 0.0 copy-done
  395.7 2.6 fusion.7
  (4 shorter events, 0.0 us)
Async XLA Ops:
  6.5 42.2 %all-gather.4.cloned.1.call-start = ((), (), s32[]{:S(2)}) async-start(), calls=%async_computation | async-start | bytes 1310720 | tf_op jit(solution)/shard_map/all_gather | solution.py:62
  6.5 3.1 copy-start.1
  9.6 18.6 %copy-start.2 = (f32[1,512]{1,0:T(1,128)S(1)}, f32[1,512]{1,0:T(1,128)}, u32[]{:S(2)}) copy-start(f32[1,512]{1,0:T(1,128)} %param.12) | copy-start | bytes 6148
  30.1 169.8 %all-gather.6.cloned.1.call-start = ((), (), s32[]{:S(2)}) async-start(), calls=%async_computation.1 | async-start | bytes 10485760 | tf_op jit(solution)/shard_map/all_gather | solution.py:67
  34.0 315.3 %all-gather.8.cloned.1.call-start = ((), (), s32[]{:S(2)}) async-start(), calls=%async_computation.2 | async-start | bytes 10485760 | tf_op jit(solution)/shard_map/all_gather | solution.py:76
  37.9 311.5 %copy-start.3 = (f32[1,2048]{1,0:T(1,128)S(1)}, f32[1,2048]{1,0:T(1,128)}, u32[]{:S(2)}) copy-start(f32[1,2048]{1,0:T(1,128)} %param.17) | copy-start | bytes 24580
  37.9 311.5 %copy-start.4 = (f32[1,2048]{1,0:T(1,128)S(1)}, f32[1,2048]{1,0:T(1,128)}, u32[]{:S(2)}) copy-start(f32[1,2048]{1,0:T(1,128)} %param.15) | copy-start | bytes 24580
  37.9 311.5 %copy-start.5 = (f32[2048]{0:T(1024)S(1)}, f32[2048]{0:T(1024)}, u32[]{:S(2)}) copy-start(f32[2048]{0:T(1024)} %param.13) | copy-start | bytes 24580
  37.9 357.8 %all-reduce.2.cloned.1.call-start = ((), (), s32[]{:S(2)}) async-start(), calls=%async_computation.3 | async-start | bytes 2097152 | tf_op jit(solution)/shard_map/psum | solution.py:81
  349.3 46.4 %copy-start = (bf16[256,2048]{1,0:T(8,128)(2,1)S(1)}, bf16[256,2048]{1,0:T(8,128)(2,1)}, u32[]{:S(2)}) copy-start(bf16[256,2048]{1,0:T(8,128)(2,1)} %all-gather.4.cloned.1.call-done) | copy-start | bytes 3145732
Sparse Core Ops, SparseCore 0:
  30.2 18.4 all-gather.3
  50.3 149.6 all-gather.5
  201.5 147.7 all-gather.7
  361.2 34.4 all-reduce.1
where the time goes:
time: 405 us
  waiting for transfers between devices  345 us (85%)
  blocking collectives  17.4 us (4%)
  other arithmetic  14.9 us (4%)
  matrix products  13.9 us (3%)
  between operations  13.2 us (3%)
    all_gather x1, waiting for transfers between devices, body(): lax.all_gather(up_weight.astype(jnp.bfloat16), 'fs', axis=0, tiled=True)  150 us
    all_gather x1, waiting for transfers between devices, body(): lax.all_gather(down_weight.astype(jnp.bfloat16), 'fs', axis=1, tiled=True)  149 us
    psum x1, waiting for transfers between devices, body(): lax.psum(partial_value.astype(jnp.bfloat16), 'tp').astype(jnp.float32)  34.6 us
    all_gather x1, blocking collectives, body(): lax.all_gather(group_weight.astype(jnp.bfloat16), 'fs', axis=0, tiled=True)  17.4 us
    dot_general x1, matrix products, body(): jnp.dot(hidden, lax.all_gather(down_weight.astype(jnp.bfloat16), 'fs', ax...  11.7 us
    all_gather x1, waiting for transfers between devices, body(): carried = lax.all_gather(carried_cols, 'tp', axis=1, tiled=True)  10.8 us
  transfers between devices with their start and end apart: 4, of which 4 were waited for; matrix products, arithmetic and copies ran while one was open for 2% of the time, Pallas kernels for 0%

commit v1 on v0

--- a/solution.py
+++ b/solution.py
@@ -1,7 +1,13 @@
+import functools
+import math
+
 import jax
 import jax.numpy as jnp
 from jax import lax
+from jax.experimental import pallas as pl
+from jax.experimental.pallas import tpu as pltpu
 from jax.sharding import PartitionSpec as P
+
 
 GROUPS = 4
 LENGTH = 128
@@ -29,7 +35,7 @@
     )
 
 
-def body(
+def gather_body(
     tokens,
     mix_gain,
     group_weight,
@@ -82,6 +88,293 @@
     return (carried.astype(jnp.float32) + summed).astype(jnp.bfloat16)
 
 
+def bits_of(count):
+    return [1 << b for b in range(count.bit_length() - 1)]
+
+
+def local(kernel, outs, scalars, *arrays, scratch=(), flops=0):
+    moved = sum(a.size * a.dtype.itemsize for a in (*arrays, *outs))
+    held = moved + sum(math.prod(shape) * jnp.dtype(kind).itemsize for shape, kind in scratch)
+    return pl.pallas_call(
+        kernel,
+        out_shape=outs,
+        in_specs=[pl.BlockSpec(memory_space=pltpu.SMEM)]
+        + [pl.BlockSpec(memory_space=pltpu.VMEM)] * len(arrays),
+        out_specs=[pl.BlockSpec(memory_space=pltpu.VMEM)] * len(outs),
+        scratch_shapes=[pltpu.VMEM(shape, kind) for shape, kind in scratch],
+        compiler_params=pltpu.CompilerParams(vmem_limit_bytes=min(3 * held + (8 << 20), 60 << 20)),
+        cost_estimate=pl.CostEstimate(flops=max(flops, 1 << 20), bytes_accessed=moved, transcendentals=0),
+    )(jnp.stack([jnp.int32(v) for v in scalars]), *arrays)
+
+
+def array(shape, kind=jnp.bfloat16):
+    return jax.ShapeDtypeStruct(shape, kind)
+
+
+def at(index, size):
+    return pl.ds(pl.multiple_of(index * size, size), size)
+
+
+def prep_kernel(scalars, tokens, packed):
+    rows, width = tokens.shape[0], packed.shape[1]
+    promoted = tokens[...].astype(jnp.float32)
+    inverse = lax.rsqrt(jnp.mean(promoted * promoted, axis=-1, keepdims=True) + norm_eps)
+    lane = lax.broadcasted_iota(jnp.int32, (rows, 128), 1)
+    pieces = jnp.zeros((rows, 128), jnp.float32)
+    for place in range(3):
+        piece = inverse.astype(jnp.bfloat16).astype(jnp.float32)
+        pieces = jnp.where(lane == place, piece, pieces)
+        inverse = inverse - piece
+    packed[:rows, :] = tokens[:, at(scalars[0], width)]
+    packed[rows:, :] = jnp.zeros((packed.shape[0] - rows, width), jnp.bfloat16)
+    packed[rows:, :rows] = jnp.transpose(pieces)[: packed.shape[0] - rows].astype(jnp.bfloat16)
+
+
+def mix_kernel(scalars, packed, gain, scale, *refs):
+    *pieces, carried, mixer = refs
+    rows, depth = carried.shape[0], pieces[0].shape[0]
+    for d, piece in enumerate(pieces):
+        mixer[at(scalars[0] ^ d, depth), :] = piece[...]
+    tokens = packed[:rows, :].astype(jnp.float32)
+    three = packed[rows:, :rows].astype(jnp.float32)
+    inverse = three[0:1] + three[1:2] + three[2:3]
+    inverse = jnp.transpose(jnp.broadcast_to(inverse, (128, rows)))[:, :1]
+    normed = (tokens * inverse * gain[...]).astype(jnp.bfloat16)
+    window = jnp.left_shift(jnp.int32(2), scalars[1])
+    row = lax.broadcasted_iota(jnp.int32, (LENGTH, LENGTH), 0)
+    offset = row - lax.broadcasted_iota(jnp.int32, (LENGTH, LENGTH), 1)
+    band = jnp.where((offset >= 0) & (offset < window), 1.0, 0.0).astype(jnp.bfloat16)
+    position = lax.broadcasted_iota(jnp.int32, (LENGTH, 1), 0)
+    divisor = jnp.minimum(position + 1, window).astype(jnp.float32)
+    for first in range(0, rows, LENGTH):
+        here = slice(first, first + LENGTH)
+        summed = jnp.dot(band, normed[here], preferred_element_type=jnp.float32)
+        pooled = (summed / divisor - normed[here].astype(jnp.float32)).astype(jnp.bfloat16)
+        mixed = jnp.dot(pooled, mixer[...], preferred_element_type=jnp.float32) * scale[...]
+        carried[here, :] = (tokens[here] + mixed).astype(jnp.bfloat16)
+
+
+def norm_kernel(scalars, gain, *refs):
+    *columns, normed, kept = refs
+    rows, width = columns[0].shape
+    total = jnp.zeros((rows, 1), jnp.float32)
+    for column in columns:
+        value = column[...].astype(jnp.float32)
+        total = total + jnp.sum(value * value, axis=-1, keepdims=True)
+    inverse = lax.rsqrt(total / (width * len(columns)) + norm_eps)
+    for e, column in enumerate(columns):
+        place = at(scalars[0] ^ e, width)
+        value = column[...].astype(jnp.float32) * inverse * gain[:, place]
+        normed[:, place] = value.astype(jnp.bfloat16)
+        kept[:, place] = column[at(scalars[1], kept.shape[0]), :]
+
+
+def up_kernel(scalars, scale, *refs, n, reps):
+    normed, pieces, (hidden, weight) = refs[:n], refs[n:-2], refs[-2:]
+    rows = normed[0].shape[0]
+    own, pieces = pieces[0], pieces[1:]
+    depth = own.shape[0]
+    weight[at(scalars[0], depth), :] = own[...]
+    for place, piece in enumerate(pieces):
+        d, k = place // reps + 1, place % reps
+        part = lax.rem(scalars[1] - k + reps, reps)
+        weight[at((scalars[0] ^ d) * reps + part, depth // reps), :] = piece[...]
+    for d in range(n):
+        value = jnp.dot(normed[d][...], weight[...], preferred_element_type=jnp.float32)
+        value = jnp.maximum(value * scale[...], 0.0)
+        hidden[d * rows : (d + 1) * rows, :] = (value * value).astype(jnp.bfloat16)
+
+
+def down_kernel(scalars, hidden, scale, *refs, n):
+    *pieces, stays, goes, weight = refs
+    size = weight.shape[0] // len(pieces)
+    for k, piece in enumerate(pieces):
+        part = lax.rem(scalars[0] - k + len(pieces), len(pieces))
+        weight[at(part, size), :] = piece[...]
+    half = stays.shape[0] // n
+    for b in range(n):
+        for out, side in ((goes, 1 - scalars[1]), (stays, scalars[1])):
+            value = jnp.dot(
+                hidden[at(2 * b + side, half), :], weight[...], preferred_element_type=jnp.float32
+            )
+            out[b * half : (b + 1) * half, :] = (value * scale[...]).astype(jnp.bfloat16)
+
+
+def fold_kernel(scalars, stayed, got, stays, goes, *, n):
+    half = stays.shape[0] // n
+    for b in range(n):
+        for out, side in ((goes, 1 - scalars[0]), (stays, scalars[0])):
+            place = at(2 * b + side, half)
+            value = stayed[place, :].astype(jnp.float32) + got[place, :].astype(jnp.float32)
+            out[b * half : (b + 1) * half, :] = value.astype(jnp.bfloat16)
+
+
+def sum_kernel(scalars, *refs, n):
+    del scalars
+    pairs, outs = refs[:-n], refs[-n:]
+    rows, width = outs[0].shape[0], pairs[0].shape[1]
+    for c in range(len(pairs) // 2):
+        stayed, got = pairs[2 * c], pairs[2 * c + 1]
+        for e, out in enumerate(outs):
+            here = slice(e * rows, (e + 1) * rows)
+            value = stayed[here, :].astype(jnp.float32) + got[here, :].astype(jnp.float32)
+            out[:, c * width : (c + 1) * width] = value.astype(jnp.bfloat16)
+
+
+def final_kernel(scalars, kept, *refs, n):
+    *sums, out = refs
+    width = out.shape[1] // n
+    groups = len(sums) // n
+    for q in range(n):
+        place = at(scalars[0] ^ q, width)
+        value = kept[:, place].astype(jnp.float32)
+        for e in range(n):
+            side, column = divmod(q ^ e, n // groups)
+            piece = sums[side * n + e][:, column * width : (column + 1) * width]
+            value = value + piece.astype(jnp.float32)
+        out[:, place] = value.astype(jnp.bfloat16)
+
+
+def place_kernel(scalars, *refs):
+    *parts, out = refs
+    for e, part in enumerate(parts):
+        out[at(scalars[e], part.shape[0]), :] = part[...]
+
+
+def exchange_body(sizes):
+    reps, n, m = sizes["rep"], sizes["fs"], sizes["tp"]
+    axes = ("rep", "fs", "tp")
+    tp_bits = bits_of(m)
+
+    def hop(values, rep=0, fs=0, tp=0):
+        pairs = []
+        for a in range(reps):
+            for b in range(n):
+                for c in range(m):
+                    target = (((a + rep) % reps) * n + (b ^ fs)) * m + (c ^ tp)
+                    pairs.append(((a * n + b) * m + c, target))
+        return lax.ppermute(values, axes, pairs)
+
+    def spread_fs(own):
+        held = [own]
+        for d in range(1, n):
+            low = d & -d
+            held.append(hop(held[d ^ low], fs=low))
+        return held
+
+    def gather_tp(own):
+        held = {0: own}
+        for bit in reversed(tp_bits):
+            for e in list(held):
+                held[e ^ bit] = hop(held[e], tp=bit)
+        return [held[e] for e in range(m)]
+
+    def rank_of_rows(j):
+        place = 0
+        for bit in tp_bits:
+            place = 2 * place + (j // bit) % 2
+        return place
+
+    def body(
+        tokens,
+        mix_gain,
+        group_weight,
+        group_scale,
+        mlp_gain,
+        up_weight,
+        up_scale,
+        down_weight,
+        down_scale,
+    ):
+        rows, model_width = tokens.shape
+        r, i, j = (lax.axis_index(axis) for axis in axes)
+        width = group_weight.shape[1]
+        units = up_weight.shape[1] // n
+        cols = down_weight.shape[1]
+
+        mixer = spread_fs(group_weight.astype(jnp.bfloat16))
+        (packed,) = local(prep_kernel, [array((rows + 16, width))], [j], tokens)
+        blocks = spread_fs(packed)
+
+        def send_parts(block_of):
+            got = [[block_of(0).astype(jnp.bfloat16)]]
+            for d in range(1, n):
+                block = block_of(d)
+                part = block.shape[0] // reps
+                part = lax.dynamic_slice_in_dim(block, r * part, part, 0).astype(jnp.bfloat16)
+                part = hop(part, fs=d)
+                got.append([part] + [hop(part, rep=k) for k in range(1, reps)])
+            return got
+
+        ups = send_parts(lambda d: lax.dynamic_slice_in_dim(up_weight, (i ^ d) * units, units, 1))
+        downs = send_parts(lambda d: lax.dynamic_slice_in_dim(down_weight, (i ^ d) * units, units, 0))
+
+        gain = lax.dynamic_slice_in_dim(mix_gain.reshape(1, -1), j * width, width, 1)
+        normed, kept = [], None
+        part_rows = rows // m
+        for d in range(n):
+            (carried,) = local(
+                mix_kernel, [array((rows, width))], [i, j],
+                blocks[d], gain, group_scale, *mixer,
+                scratch=[((n * group_weight.shape[0], width), jnp.bfloat16)],
+                flops=2 * rows * width * (width + LENGTH),
+            )
+            columns = gather_tp(carried)
+            value, part = local(
+                norm_kernel, [array((rows, model_width)), array((part_rows, model_width))],
+                [j, rank_of_rows(j)], mlp_gain.reshape(1, -1), *columns,
+                flops=10 * rows * model_width,
+            )
+            normed.append(value)
+            kept = part if d == 0 else kept
+        (hidden,) = local(
+            functools.partial(up_kernel, n=n, reps=reps), [array((n * rows, units))], [i, r],
+            lax.dynamic_slice_in_dim(up_scale, i * units, units, 1),
+            *normed, *(p for block in ups for p in block),
+            scratch=[((model_width, units), jnp.bfloat16)],
+            flops=2 * n * rows * model_width * units,
+        )
+
+        sums = []
+        for d in range(n):
+            scale = lax.dynamic_slice_in_dim(down_scale, (i ^ d) * cols, cols, 1)
+            half = array((n * rows // 2, cols))
+            stays, goes = local(
+                functools.partial(down_kernel, n=n), [half, half], [r, j % 2],
+                hidden, scale, *downs[d],
+                scratch=[((units, cols), jnp.bfloat16)],
+                flops=2 * n * rows * units * cols,
+            )
+            for bit in tp_bits[1:]:
+                got = hop(goes, tp=bit // 2)
+                half = array((half.shape[0] // 2, cols))
+                stays, goes = local(
+                    functools.partial(fold_kernel, n=n), [half, half],
+                    [(j // bit) % 2], stays, got,
+                )
+            sums += [stays, hop(goes, tp=tp_bits[-1])]
+        terms = []
+        for side in range(2):
+            mine = sums[side * n : (side + 1) * n]
+            outs = local(
+                functools.partial(sum_kernel, n=n),
+                [array((part_rows, cols * n // 2))] * n, [i], *mine,
+            )
+            terms += [outs[0]] + [hop(outs[e], fs=e) for e in range(1, n)]
+        (out,) = local(
+            functools.partial(final_kernel, n=n), [array((part_rows, model_width))], [i],
+            kept, *terms,
+        )
+        parts = gather_tp(out)
+        (out,) = local(
+            place_kernel, [array((rows, model_width))],
+            [rank_of_rows(j ^ e) for e in range(m)], *parts,
+        )
+        return out
+
+    return body
+
+
 def solution(mesh):
     in_specs = (
         P(("rep", "fs"), None),
@@ -95,4 +388,17 @@
         P(),
     )
     out_specs = P(("rep", "fs"), None)
-    return jax.shard_map(body, mesh=mesh, in_specs=in_specs, out_specs=out_specs, check_vma=False)
+    sizes = dict(mesh.shape)
+
+    def layer(*args):
+        tokens, up = args[0], args[5]
+        moved = up.size // sizes["tp"]
+        gathered = tokens.size // sizes["rep"]
+        powers = all(sizes[a] & (sizes[a] - 1) == 0 for a in ("fs", "tp"))
+        fits = sizes["tp"] == sizes["fs"] == GROUPS
+        chosen = exchange_body(sizes) if powers and fits and gathered < moved else gather_body
+        return jax.shard_map(
+            chosen, mesh=mesh, in_specs=in_specs, out_specs=out_specs, check_vma=False
+        )(*args)
+
+    return layer

time: 405 us -> 175 us (0.43)
  waiting for transfers between devices: 345 us -> 91 us
  starting transfers between devices: 0.13 us -> 47.4 us
  Pallas kernels: 0 us -> 23.9 us
  blocking collectives: 17.4 us -> 0 us
  matrix products: 13.9 us -> 0 us
  other arithmetic: 14.9 us -> 1.36 us
  between operations: 13.2 us -> 0.28 us
  local copies, waits for them, and re-layouts: 0.78 us -> 10.4 us
    all_gather x3 -> x0, waiting for transfers between devices: 310 us -> none  [the longest x1 150 us: body(): lax.all_gather(up_weight.astype(jnp.bfloat16), 'fs', axis=0, tiled=True)]
    ppermute x0 -> x47, waiting for transfers between devices: none -> 91 us  [hop(): return lax.ppermute(values, axes, pairs)]
    ppermute x0 -> x47, starting transfers between devices: none -> 47.4 us  [hop(): return lax.ppermute(values, axes, pairs)]
    psum x1 -> x0, waiting for transfers between devices: 34.6 us -> none  [body(): lax.psum(partial_value.astype(jnp.bfloat16), 'tp').astype(jnp.float32)]
    pallas_call x0 -> x22, Pallas kernels: none -> 23.9 us  [local(): pl.pallas_call(kernel, out_shape=outs, in_specs=[pl.BlockSpec(memory_spac...]
    all_gather x1 -> x0, blocking collectives: 17.4 us -> none  [body(): lax.all_gather(group_weight.astype(jnp.bfloat16), 'fs', axis=0, tiled=True)]
    dot_general x3 -> x0, matrix products: 13.9 us -> none  [the longest x1 11.7 us: body(): jnp.dot(hidden, lax.all_gather(down_weight.astype(jnp.bfloat16), 'fs', ax...]
    convert_element_type x7 -> x1, other arithmetic: 11.8 us -> 0.98 us  [body(): mixer = spread_fs(group_weight.astype(jnp.bfloat16))]
  transfers between devices with their start and end apart: 4 -> 47, of which waited for: 4 -> 19; matrix products, arithmetic and copies ran while one was open for 2% -> 5% of each run, Pallas kernels for 0% -> 13%
where the time goes in v1:
time: 175 us; the launch traced here: 174 us
  waiting for transfers between devices  91 us (52%)
  starting transfers between devices  47.4 us (27%)
  Pallas kernels  23.9 us (14%)
  local copies, waits for them, and re-layouts  10.4 us (6%)
    ppermute x47, waiting for transfers between devices, hop(): return lax.ppermute(values, axes, pairs)  91 us
    ppermute x47, starting transfers between devices, hop(): return lax.ppermute(values, axes, pairs)  47.4 us
    pallas_call x22, Pallas kernels, local(): pl.pallas_call(kernel, out_shape=outs, in_specs=[pl.BlockSpec(memory_spac...  23.9 us
  transfers between devices with their start and end apart: 47, of which 19 were waited for; matrix products, arithmetic and copies ran while one was open for 5% of the time, Pallas kernels for 13%

profile of v1, /device:TPU:0, one launch (start us, length us, event | category | flops | bytes accessed | tf_op | source)
XLA Modules:
  0.0 174.2 jit_solution(17636220763949274363)
XLA Ops:
  0.0 1.0 convert_element_type.27.refs_0_
  1.0 3.1 %collective-permute-start = (bf16[128,512]{1,0:T(8,128)(2,1)S(1)}, bf16[128,512]{1,0:T(8,128)(2,1)S(1)}, u32[]{:S(2)}, u32[]{:S(2)}) collective-permute-start(bf16[128,512]{1,0:T(8,128)(2,1)S(1)} %convert_element_type.27.refs_0_), channel_id=1, source_target_pairs={{0,4},{1,5},{2,6},{3,7},{4,0},{5,1},{6,2},{7,3},{8,12},{9,13},{10,... | collective-permute-start | bytes 393224 | tf_op jit(solution)/shard_map/ppermute | solution.py:256
  4.1 2.6 %collective-permute-start.1 = (bf16[128,512]{1,0:T(8,128)(2,1)S(1)}, bf16[128,512]{1,0:T(8,128)(2,1)S(1)}, u32[]{:S(2)}, u32[]{:S(2)}) collective-permute-start(bf16[128,512]{1,0:T(8,128)(2,1)S(1)} %convert_element_type.27.refs_0_), channel_id=1, source_target_pairs={{0,8},{1,9},{2,10},{3,11},{4,12},{5,13},{6,14},{7,15},{8,0},{9,1},... | collective-permute-start | bytes 393224 | tf_op jit(solution)/shard_map/ppermute | solution.py:256
  6.7 1.2 copy-done
  8.6 1.8 %fusion = (bf16[256,512]{1,0:T(8,128)(2,1)S(1)}, bf16[256,512]{1,0:T(8,128)(2,1)S(1)}, bf16[256,512]{1,0:T(8,128)(2,1)S(1)}) fusion(f32[512,2048]{1,0:T(8,128)} %param.14, s32[]{:T(128)S(6)} %select_n.151, s32[]{:T(128)S(6)} %select_n.157, s32[]{:T(128)S(6)} %select_n.153, s32[]{:T(128)S(6)} %select_n.155), kind=kLoop, calls=%fused_computation.18 | loop fusion | bytes 1572880 | tf_op jit(solution)/shard_map/dynamic_slice | solution.py:304
  10.7 2.9 %collective-permute-start.20 = (bf16[256,512]{1,0:T(8,128)(2,1)S(1)}, bf16[256,512]{1,0:T(8,128)(2,1)}, u32[]{:S(2)}, u32[]{:S(2)}) collective-permute-start(bf16[256,512]{1,0:T(8,128)(2,1)S(1)} %get-tuple-element.68), channel_id=1, source_target_pairs={{0,8},{1,9},{2,10},{3,11},{4,12},{5,13},{6,14},{7,15},{8,0},{9,1},... | collective-permute-start | bytes 786440 | tf_op jit(solution)/shard_map/ppermute | solution.py:256
  13.6 1.3 collective-permute-start.22
  14.9 3.1 %collective-permute-done.1.refs_2_ = bf16[128,512]{1,0:T(8,128)(2,1)S(1)} collective-permute-done((bf16[128,512]{1,0:T(8,128)(2,1)S(1)}, bf16[128,512]{1,0:T(8,128)(2,1)S(1)}, u32[]{:S(2)}, u32[]{:S(2)}) %collective-permute-start.1) | collective-permute-done | bytes 131104 | tf_op jit(solution)/shard_map/ppermute | solution.py:256
  18.1 1.6 collective-permute-start.2
  19.6 2.3 %dynamic-slice_convert_fusion.2 = (bf16[256,512]{1,0:T(8,128)(2,1)}, bf16[256,512]{1,0:T(8,128)(2,1)S(1)}, bf16[256,512]{1,0:T(8,128)(2,1)S(1)}) fusion(f32[2048,512]{1,0:T(8,128)} %param.16, s32[]{:T(128)S(6)} %dynamic_slice.72, s32[]{:T(128)S(6)} %dynamic_slice.66, s32[]{:T(128)S(6)} %dynamic_slice.69), kind=kLoop, calls=%fused_computation.2 | loop fusion | bytes 1572876 | tf_op jit(solution)/shard_map/convert_element_type | solution.py:304
  21.9 13.5 %collective-permute-done.2.refs_3_ = bf16[128,512]{1,0:T(8,128)(2,1)S(1)} collective-permute-done((bf16[128,512]{1,0:T(8,128)(2,1)S(1)}, bf16[128,512]{1,0:T(8,128)(2,1)S(1)}, u32[]{:S(2)}, u32[]{:S(2)}) %collective-permute-start.2) | collective-permute-done | bytes 131104 | tf_op jit(solution)/shard_map/ppermute | solution.py:256
  35.4 2.5 %collective-permute-start.6 = (bf16[272,512]{1,0:T(8,128)(2,1)S(1)}, bf16[272,512]{1,0:T(8,128)(2,1)S(1)}, u32[]{:S(2)}, u32[]{:S(2)}) collective-permute-start(bf16[272,512]{1,0:T(8,128)(2,1)S(1)} %shard_map.91.packed), channel_id=1, source_target_pairs={{0,4},{1,5},{2,6},{3,7},{4,0},{5,1},{6,2},{7,3},{8,12},{9,13},{10,... | collective-permute-start | bytes 835592 | tf_op jit(solution)/shard_map/ppermute | solution.py:256
  38.0 0.8 dynamic-slice.3
  38.7 1.3 shard_map.92.refs_0_
  40.0 2.1 %collective-permute-start.26 = (bf16[256,512]{1,0:T(8,128)(2,1)S(1)}, bf16[256,512]{1,0:T(8,128)(2,1)S(1)}, u32[]{:S(2)}, u32[]{:S(2)}) collective-permute-start(bf16[256,512]{1,0:T(8,128)(2,1)S(1)} %get-tuple-element.64), channel_id=1, source_target_pairs={{0,4},{1,5},{2,6},{3,7},{4,0},{5,1},{6,2},{7,3},{8,12},{9,13},{10,... | collective-permute-start | bytes 786440 | tf_op jit(solution)/shard_map/ppermute | solution.py:256
  42.1 1.1 collective-permute-start.33
  43.2 10.1 %collective-permute-done.6.packed = bf16[272,512]{1,0:T(8,128)(2,1)S(1)} collective-permute-done((bf16[272,512]{1,0:T(8,128)(2,1)S(1)}, bf16[272,512]{1,0:T(8,128)(2,1)S(1)}, u32[]{:S(2)}, u32[]{:S(2)}) %collective-permute-start.6) | collective-permute-done | bytes 278560 | tf_op jit(solution)/shard_map/ppermute | solution.py:256
  53.3 1.5 collective-permute-start.4
  54.8 1.3 shard_map.96.refs_0_
  56.1 1.3 shard_map.94.refs_0_
  57.4 7.4 %collective-permute-done.26.refs_0_ = bf16[256,512]{1,0:T(8,128)(2,1)S(1)} collective-permute-done((bf16[256,512]{1,0:T(8,128)(2,1)S(1)}, bf16[256,512]{1,0:T(8,128)(2,1)S(1)}, u32[]{:S(2)}, u32[]{:S(2)}) %collective-permute-start.26) | collective-permute-done | bytes 262176 | tf_op jit(solution)/shard_map/ppermute | solution.py:256
  64.9 1.6 collective-permute-start.8
  67.0 1.3 shard_map.98.refs_0_
  68.3 1.6 collective-permute-start.16
  70.1 4.0 %collective-permute-done.8.refs_2_ = bf16[256,512]{1,0:T(8,128)(2,1)S(1)} collective-permute-done((bf16[256,512]{1,0:T(8,128)(2,1)S(1)}, bf16[256,512]{1,0:T(8,128)(2,1)S(1)}, u32[]{:S(2)}, u32[]{:S(2)}) %collective-permute-start.8) | collective-permute-done | bytes 262176 | tf_op jit(solution)/shard_map/ppermute | solution.py:256
  74.1 5.6 %collective-permute-done.12.refs_2_ = bf16[256,512]{1,0:T(8,128)(2,1)S(1)} collective-permute-done((bf16[256,512]{1,0:T(8,128)(2,1)S(1)}, bf16[256,512]{1,0:T(8,128)(2,1)S(1)}, u32[]{:S(2)}, u32[]{:S(2)}) %collective-permute-start.12) | collective-permute-done | bytes 262176 | tf_op jit(solution)/shard_map/ppermute | solution.py:256
  80.2 0.7 constant_dynamic-slice_fusion
  80.9 1.3 dynamic-slice_convert_fusion.1.refs_4_
  82.3 2.5 %collective-permute-done.16.refs_2_ = bf16[256,512]{1,0:T(8,128)(2,1)S(1)} collective-permute-done((bf16[256,512]{1,0:T(8,128)(2,1)S(1)}, bf16[256,512]{1,0:T(8,128)(2,1)S(1)}, u32[]{:S(2)}, u32[]{:S(2)}) %collective-permute-start.16) | collective-permute-done | bytes 262176 | tf_op jit(solution)/shard_map/ppermute | solution.py:256
  84.9 2.5 %collective-permute-start.37 = (bf16[256,512]{1,0:T(8,128)(2,1)}, bf16[256,512]{1,0:T(8,128)(2,1)S(1)}, u32[]{:S(2)}, u32[]{:S(2)}) collective-permute-start(bf16[256,512]{1,0:T(8,128)(2,1)} %get-tuple-element.63), channel_id=1, source_target_pairs={{0,12},{1,13},{2,14},{3,15},{4,8},{5,9},{6,10},{7,11},{8,4},{9,5},... | collective-permute-start | bytes 786440 | tf_op jit(solution)/shard_map/ppermute | solution.py:256
  87.4 1.5 collective-permute-start.19
  89.4 1.5 collective-permute-start.23
  91.0 1.3 dynamic-slice_convert_fusion.refs_0_
  92.9 1.5 shard_map.93
  94.5 2.1 %shard_map.95 = (bf16[256,2048]{1,0:T(8,128)(2,1)S(1)}, bf16[64,2048]{1,0:T(8,128)(2,1)}) custom-call(s32[2]{0:T(128)S(1)} %pad_add_fusion.1.scalars, f32[1,2048]{1,0:T(1,128)S(1)} %bitcast.12, bf16[256,512]{1,0:T(8,128)(2,1)S(1)} %shard_map.94.refs_0_, bf16[256,512]{1,0:T(8,128)(2,1)S(1)} %collective-permute-done.7.refs_1_, ...), custom_call_target="tpu_custom_call" | custom-call | flops 5242880 | bytes 2367488 | tf_op jit(solution)/shard_map/pallas_call | solution.py:98
  96.5 1.7 shard_map.97
  98.2 0.9 copy-done.2
  99.1 1.7 shard_map.99
  100.8 1.5 collective-permute-start.34
  102.8 5.1 %collective-permute-done.23.refs_10_ = bf16[256,512]{1,0:T(8,128)(2,1)S(1)} collective-permute-done((bf16[256,512]{1,0:T(8,128)(2,1)}, bf16[256,512]{1,0:T(8,128)(2,1)S(1)}, u32[]{:S(2)}, u32[]{:S(2)}) %collective-permute-start.23) | collective-permute-done | bytes 262176 | tf_op jit(solution)/shard_map/ppermute | solution.py:256
  108.0 3.6 %shard_map.100.hidden = bf16[1024,512]{1,0:T(8,128)(2,1)S(1)} custom-call(s32[2]{0:T(128)S(1)} %pad_add_fusion.4.scalars, f32[1,512]{1,0:T(1,128)S(1)} %get-tuple-element.73.scale, bf16[256,2048]{1,0:T(8,128)(2,1)S(1)} %get-tuple-element.35.refs_0_, bf16[256,2048]{1,0:T(8,128)(2,1)S(1)} %get-tuple-element.36.refs_1_, ...), custom_call_target="tpu_custom_call" | custom-call | flops 2147483648 | bytes 7342080 | tf_op jit(solution)/shard_map/pallas_call | solution.py:98
  111.6 1.3 shard_map.101
  113.0 0.6 collective-permute-done.27.refs_1_
  113.6 1.3 shard_map.103
  115.0 4.2 %collective-permute-done.34.refs_1_ = bf16[256,512]{1,0:T(8,128)(2,1)S(1)} collective-permute-done((bf16[256,512]{1,0:T(8,128)(2,1)S(1)}, bf16[256,512]{1,0:T(8,128)(2,1)S(1)}, u32[]{:S(2)}, u32[]{:S(2)}) %collective-permute-start.34) | collective-permute-done | bytes 262176 | tf_op jit(solution)/shard_map/ppermute | solution.py:256
  119.2 1.3 shard_map.106
  120.6 3.5 %collective-permute-done.38.refs_1_ = bf16[256,512]{1,0:T(8,128)(2,1)S(1)} collective-permute-done((bf16[256,512]{1,0:T(8,128)(2,1)S(1)}, bf16[256,512]{1,0:T(8,128)(2,1)S(1)}, u32[]{:S(2)}, u32[]{:S(2)}) %collective-permute-start.38) | collective-permute-done | bytes 262176 | tf_op jit(solution)/shard_map/ppermute | solution.py:256
  124.1 1.5 shard_map.108
  125.8 1.6 collective-permute-start.25
  128.2 1.6 collective-permute-start.36
  130.5 4.5 %collective-permute-done.25.refs_1_ = bf16[256,512]{1,0:T(8,128)(2,1)S(1)} collective-permute-done((bf16[256,512]{1,0:T(8,128)(2,1)S(1)}, bf16[256,512]{1,0:T(8,128)(2,1)S(1)}, u32[]{:S(2)}, u32[]{:S(2)}) %collective-permute-start.25) | collective-permute-done | bytes 262176 | tf_op jit(solution)/shard_map/ppermute | solution.py:256
  135.1 5.6 %collective-permute-done.29.refs_3_ = bf16[256,512]{1,0:T(8,128)(2,1)S(1)} collective-permute-done((bf16[256,512]{1,0:T(8,128)(2,1)S(1)}, bf16[256,512]{1,0:T(8,128)(2,1)S(1)}, u32[]{:S(2)}, u32[]{:S(2)}) %collective-permute-start.29) | collective-permute-done | bytes 262176 | tf_op jit(solution)/shard_map/ppermute | solution.py:256
  140.9 1.9 %collective-permute-start.31 = (bf16[64,1024]{1,0:T(8,128)(2,1)S(1)}, bf16[64,1024]{1,0:T(8,128)(2,1)S(1)}, u32[]{:S(2)}, u32[]{:S(2)}) collective-permute-start(bf16[64,1024]{1,0:T(8,128)(2,1)S(1)} %get-tuple-element.49), channel_id=1, source_target_pairs={{0,8},{1,9},{2,10},{3,11},{4,12},{5,13},{6,14},{7,15},{8,0},{9,1},... | collective-permute-start | bytes 393224 | tf_op jit(solution)/shard_map/ppermute | solution.py:256
  142.8 2.5 %collective-permute-start.32 = (bf16[64,1024]{1,0:T(8,128)(2,1)S(1)}, bf16[64,1024]{1,0:T(8,128)(2,1)S(1)}, u32[]{:S(2)}, u32[]{:S(2)}) collective-permute-start(bf16[64,1024]{1,0:T(8,128)(2,1)S(1)} %get-tuple-element.50), channel_id=1, source_target_pairs={{0,12},{1,13},{2,14},{3,15},{4,8},{5,9},{6,10},{7,11},{8,4},{9,5},... | collective-permute-start | bytes 393224 | tf_op jit(solution)/shard_map/ppermute | solution.py:256
  145.2 1.0 collective-permute-done.36.refs_1_
  146.3 5.1 %collective-permute-done.40.refs_3_ = bf16[256,512]{1,0:T(8,128)(2,1)S(1)} collective-permute-done((bf16[256,512]{1,0:T(8,128)(2,1)S(1)}, bf16[256,512]{1,0:T(8,128)(2,1)S(1)}, u32[]{:S(2)}, u32[]{:S(2)}) %collective-permute-start.40) | collective-permute-done | bytes 262176 | tf_op jit(solution)/shard_map/ppermute | solution.py:256
  151.6 1.9 %collective-permute-start.42 = (bf16[64,1024]{1,0:T(8,128)(2,1)S(1)}, bf16[64,1024]{1,0:T(8,128)(2,1)S(1)}, u32[]{:S(2)}, u32[]{:S(2)}) collective-permute-start(bf16[64,1024]{1,0:T(8,128)(2,1)S(1)} %get-tuple-element.61), channel_id=1, source_target_pairs={{0,8},{1,9},{2,10},{3,11},{4,12},{5,13},{6,14},{7,15},{8,0},{9,1},... | collective-permute-start | bytes 393224 | tf_op jit(solution)/shard_map/ppermute | solution.py:256
  153.5 2.5 %collective-permute-start.43 = (bf16[64,1024]{1,0:T(8,128)(2,1)S(1)}, bf16[64,1024]{1,0:T(8,128)(2,1)S(1)}, u32[]{:S(2)}, u32[]{:S(2)}) collective-permute-start(bf16[64,1024]{1,0:T(8,128)(2,1)S(1)} %get-tuple-element.62), channel_id=1, source_target_pairs={{0,12},{1,13},{2,14},{3,15},{4,8},{5,9},{6,10},{7,11},{8,4},{9,5},... | collective-permute-start | bytes 393224 | tf_op jit(solution)/shard_map/ppermute | solution.py:256
  156.0 2.3 %collective-permute-done.41.refs_5_ = bf16[64,1024]{1,0:T(8,128)(2,1)S(1)} collective-permute-done((bf16[64,1024]{1,0:T(8,128)(2,1)S(1)}, bf16[64,1024]{1,0:T(8,128)(2,1)S(1)}, u32[]{:S(2)}, u32[]{:S(2)}) %collective-permute-start.41) | collective-permute-done | bytes 131104 | tf_op jit(solution)/shard_map/ppermute | solution.py:256
  158.3 6.1 %collective-permute-done.42.refs_6_ = bf16[64,1024]{1,0:T(8,128)(2,1)S(1)} collective-permute-done((bf16[64,1024]{1,0:T(8,128)(2,1)S(1)}, bf16[64,1024]{1,0:T(8,128)(2,1)S(1)}, u32[]{:S(2)}, u32[]{:S(2)}) %collective-permute-start.42) | collective-permute-done | bytes 131104 | tf_op jit(solution)/shard_map/ppermute | solution.py:256
  164.7 1.6 collective-permute-start.45
  166.2 4.9 %collective-permute-done.45.refs_2_ = bf16[64,2048]{1,0:T(8,128)(2,1)S(1)} collective-permute-done((bf16[64,2048]{1,0:T(8,128)(2,1)S(1)}, bf16[64,2048]{1,0:T(8,128)(2,1)S(1)}, u32[]{:S(2)}, u32[]{:S(2)}) %collective-permute-start.45) | collective-permute-done | bytes 262176 | tf_op jit(solution)/shard_map/ppermute | solution.py:256
  171.2 1.5 collective-permute-done.46.refs_3_
  172.6 1.6 shard_map.112
  (84 shorter events, 6.9 us)
Async XLA Ops:
  0.0 38.7 %copy-start.4 = (f32[1,512]{1,0:T(1,128)S(1)}, f32[1,512]{1,0:T(1,128)}, u32[]{:S(2)}) copy-start(f32[1,512]{1,0:T(1,128)} %scale.7) | copy-start | bytes 6148
  1.0 12.6 %collective-permute-start = (bf16[128,512]{1,0:T(8,128)(2,1)S(1)}, bf16[128,512]{1,0:T(8,128)(2,1)S(1)}, u32[]{:S(2)}, u32[]{:S(2)}) collective-permute-start(bf16[128,512]{1,0:T(8,128)(2,1)S(1)} %convert_element_type.27.refs_0_), channel_id=1, source_target_pairs={{0,4},{1,5},{2,6},{3,7},{4,0},{5,1},{6,2},{7,3},{8,12},{9,13},{10,... | collective-permute-start | bytes 393224 | tf_op jit(solution)/shard_map/ppermute | solution.py:256
  4.1 13.9 %collective-permute-start.1 = (bf16[128,512]{1,0:T(8,128)(2,1)S(1)}, bf16[128,512]{1,0:T(8,128)(2,1)S(1)}, u32[]{:S(2)}, u32[]{:S(2)}) collective-permute-start(bf16[128,512]{1,0:T(8,128)(2,1)S(1)} %convert_element_type.27.refs_0_), channel_id=1, source_target_pairs={{0,8},{1,9},{2,10},{3,11},{4,12},{5,13},{6,14},{7,15},{8,0},{9,1},... | collective-permute-start | bytes 393224 | tf_op jit(solution)/shard_map/ppermute | solution.py:256
  6.7 1.2 copy-start
  7.9 72.3 %copy-start.9 = (f32[1,2048]{1,0:T(1,128)S(1)}, f32[1,2048]{1,0:T(1,128)}, u32[]{:S(2)}) copy-start(f32[1,2048]{1,0:T(1,128)} %param.17) | copy-start | bytes 24580
  8.3 29.7 %collective-permute-start.10 = (bf16[272,512]{1,0:T(8,128)(2,1)S(1)}, bf16[272,512]{1,0:T(8,128)(2,1)S(1)}, u32[]{:S(2)}, u32[]{:S(2)}) collective-permute-start(bf16[272,512]{1,0:T(8,128)(2,1)S(1)} %shard_map.91.packed), channel_id=1, source_target_pairs={{0,8},{1,9},{2,10},{3,11},{4,12},{5,13},{6,14},{7,15},{8,0},{9,1},... | collective-permute-start | bytes 835592 | tf_op jit(solution)/shard_map/ppermute | solution.py:256
  10.5 82.5 %copy-start.3 = (f32[2048]{0:T(1024)S(1)}, f32[2048]{0:T(1024)}, u32[]{:S(2)}) copy-start(f32[2048]{0:T(1024)} %param.13) | copy-start | bytes 24580
  10.5 29.5 %collective-permute-start.18 = (bf16[256,512]{1,0:T(8,128)(2,1)S(1)}, bf16[256,512]{1,0:T(8,128)(2,1)}, u32[]{:S(2)}, u32[]{:S(2)}) collective-permute-start(bf16[256,512]{1,0:T(8,128)(2,1)S(1)} %get-tuple-element.67), channel_id=1, source_target_pairs={{0,4},{1,5},{2,6},{3,7},{4,0},{5,1},{6,2},{7,3},{8,12},{9,13},{10,... | collective-permute-start | bytes 786440 | tf_op jit(solution)/shard_map/ppermute | solution.py:256
  10.7 31.4 %collective-permute-start.20 = (bf16[256,512]{1,0:T(8,128)(2,1)S(1)}, bf16[256,512]{1,0:T(8,128)(2,1)}, u32[]{:S(2)}, u32[]{:S(2)}) collective-permute-start(bf16[256,512]{1,0:T(8,128)(2,1)S(1)} %get-tuple-element.68), channel_id=1, source_target_pairs={{0,8},{1,9},{2,10},{3,11},{4,12},{5,13},{6,14},{7,15},{8,0},{9,1},... | collective-permute-start | bytes 786440 | tf_op jit(solution)/shard_map/ppermute | solution.py:256
  13.6 29.6 %collective-permute-start.22 = (bf16[256,512]{1,0:T(8,128)(2,1)S(1)}, bf16[256,512]{1,0:T(8,128)(2,1)}, u32[]{:S(2)}, u32[]{:S(2)}) collective-permute-start(bf16[256,512]{1,0:T(8,128)(2,1)S(1)} %get-tuple-element.66), channel_id=1, source_target_pairs={{0,12},{1,13},{2,14},{3,15},{4,8},{5,9},{6,10},{7,11},{8,4},{9,5},... | collective-permute-start | bytes 786440 | tf_op jit(solution)/shard_map/ppermute | solution.py:256
  18.1 17.3 %collective-permute-start.2 = (bf16[128,512]{1,0:T(8,128)(2,1)S(1)}, bf16[128,512]{1,0:T(8,128)(2,1)S(1)}, u32[]{:S(2)}, u32[]{:S(2)}) collective-permute-start(bf16[128,512]{1,0:T(8,128)(2,1)S(1)} %collective-permute-done.1.refs_2_), channel_id=1, source_target_pairs={{0,4},{1,5},{2,6},{3,7},{4,0},{5,1},{6,2},{7,3},{8,12},{9,13},{10,... | collective-permute-start | bytes 393224 | tf_op jit(solution)/shard_map/ppermute | solution.py:256
  35.4 17.9 %collective-permute-start.6 = (bf16[272,512]{1,0:T(8,128)(2,1)S(1)}, bf16[272,512]{1,0:T(8,128)(2,1)S(1)}, u32[]{:S(2)}, u32[]{:S(2)}) collective-permute-start(bf16[272,512]{1,0:T(8,128)(2,1)S(1)} %shard_map.91.packed), channel_id=1, source_target_pairs={{0,4},{1,5},{2,6},{3,7},{4,0},{5,1},{6,2},{7,3},{8,12},{9,13},{10,... | collective-permute-start | bytes 835592 | tf_op jit(solution)/shard_map/ppermute | solution.py:256
  38.0 29.0 %collective-permute-start.14 = (bf16[272,512]{1,0:T(8,128)(2,1)S(1)}, bf16[272,512]{1,0:T(8,128)(2,1)S(1)}, u32[]{:S(2)}, u32[]{:S(2)}) collective-permute-start(bf16[272,512]{1,0:T(8,128)(2,1)S(1)} %collective-permute-done.10.packed), channel_id=1, source_target_pairs={{0,4},{1,5},{2,6},{3,7},{4,0},{5,1},{6,2},{7,3},{8,12},{9,13},{10,... | collective-permute-start | bytes 835592 | tf_op jit(solution)/shard_map/ppermute | solution.py:256
  40.0 24.8 %collective-permute-start.26 = (bf16[256,512]{1,0:T(8,128)(2,1)S(1)}, bf16[256,512]{1,0:T(8,128)(2,1)S(1)}, u32[]{:S(2)}, u32[]{:S(2)}) collective-permute-start(bf16[256,512]{1,0:T(8,128)(2,1)S(1)} %get-tuple-element.64), channel_id=1, source_target_pairs={{0,4},{1,5},{2,6},{3,7},{4,0},{5,1},{6,2},{7,3},{8,12},{9,13},{10,... | collective-permute-start | bytes 786440 | tf_op jit(solution)/shard_map/ppermute | solution.py:256
  42.1 22.7 %collective-permute-start.33 = (bf16[256,512]{1,0:T(8,128)(2,1)S(1)}, bf16[256,512]{1,0:T(8,128)(2,1)S(1)}, u32[]{:S(2)}, u32[]{:S(2)}) collective-permute-start(bf16[256,512]{1,0:T(8,128)(2,1)S(1)} %get-tuple-element.65), channel_id=1, source_target_pairs={{0,8},{1,9},{2,10},{3,11},{4,12},{5,13},{6,14},{7,15},{8,0},{9,1},... | collective-permute-start | bytes 786440 | tf_op jit(solution)/shard_map/ppermute | solution.py:256
  43.2 23.2 %collective-permute-start.3 = (bf16[256,512]{1,0:T(8,128)(2,1)S(1)}, bf16[256,512]{1,0:T(8,128)(2,1)S(1)}, u32[]{:S(2)}, u32[]{:S(2)}) collective-permute-start(bf16[256,512]{1,0:T(8,128)(2,1)S(1)} %shard_map.92.refs_0_), channel_id=1, source_target_pairs={{0,1},{1,0},{2,3},{3,2},{4,5},{5,4},{6,7},{7,6},{8,9},{9,8},{10,11... | collective-permute-start | bytes 786440 | tf_op jit(solution)/shard_map/ppermute | solution.py:256
  53.3 14.9 %collective-permute-start.4 = (bf16[256,512]{1,0:T(8,128)(2,1)S(1)}, bf16[256,512]{1,0:T(8,128)(2,1)S(1)}, u32[]{:S(2)}, u32[]{:S(2)}) collective-permute-start(bf16[256,512]{1,0:T(8,128)(2,1)S(1)} %shard_map.92.refs_0_), channel_id=1, source_target_pairs={{0,2},{1,3},{2,0},{3,1},{4,6},{5,7},{6,4},{7,5},{8,10},{9,11},{10,... | collective-permute-start | bytes 786440 | tf_op jit(solution)/shard_map/ppermute | solution.py:256
  64.8 3.4 %copy-start.7 = (bf16[256,512]{1,0:T(8,128)(2,1)}, bf16[256,512]{1,0:T(8,128)(2,1)S(1)}, u32[]{:S(2)}) copy-start(bf16[256,512]{1,0:T(8,128)(2,1)S(1)} %collective-permute-done.26.refs_0_) | copy-start | bytes 786436
  64.8 5.0 %collective-permute-start.7 = (bf16[256,512]{1,0:T(8,128)(2,1)S(1)}, bf16[256,512]{1,0:T(8,128)(2,1)S(1)}, u32[]{:S(2)}, u32[]{:S(2)}) collective-permute-start(bf16[256,512]{1,0:T(8,128)(2,1)S(1)} %shard_map.94.refs_0_), channel_id=1, source_target_pairs={{0,1},{1,0},{2,3},{3,2},{4,5},{5,4},{6,7},{7,6},{8,9},{9,8},{10,11... | collective-permute-start | bytes 786440 | tf_op jit(solution)/shard_map/ppermute | solution.py:256
  64.8 3.4 %copy-start.5 = (bf16[256,512]{1,0:T(8,128)(2,1)}, bf16[256,512]{1,0:T(8,128)(2,1)S(1)}, u32[]{:S(2)}) copy-start(bf16[256,512]{1,0:T(8,128)(2,1)S(1)} %collective-permute-done.33.refs_0_) | copy-start | bytes 786436
  64.9 9.2 %collective-permute-start.8 = (bf16[256,512]{1,0:T(8,128)(2,1)S(1)}, bf16[256,512]{1,0:T(8,128)(2,1)S(1)}, u32[]{:S(2)}, u32[]{:S(2)}) collective-permute-start(bf16[256,512]{1,0:T(8,128)(2,1)S(1)} %shard_map.94.refs_0_), channel_id=1, source_target_pairs={{0,2},{1,3},{2,0},{3,1},{4,6},{5,7},{6,4},{7,5},{8,10},{9,11},{10,... | collective-permute-start | bytes 786440 | tf_op jit(solution)/shard_map/ppermute | solution.py:256
  66.4 13.3 %collective-permute-start.12 = (bf16[256,512]{1,0:T(8,128)(2,1)S(1)}, bf16[256,512]{1,0:T(8,128)(2,1)S(1)}, u32[]{:S(2)}, u32[]{:S(2)}) collective-permute-start(bf16[256,512]{1,0:T(8,128)(2,1)S(1)} %shard_map.96.refs_0_), channel_id=1, source_target_pairs={{0,2},{1,3},{2,0},{3,1},{4,6},{5,7},{6,4},{7,5},{8,10},{9,11},{10,... | collective-permute-start | bytes 786440 | tf_op jit(solution)/shard_map/ppermute | solution.py:256
  66.9 12.8 %collective-permute-start.11 = (bf16[256,512]{1,0:T(8,128)(2,1)S(1)}, bf16[256,512]{1,0:T(8,128)(2,1)S(1)}, u32[]{:S(2)}, u32[]{:S(2)}) collective-permute-start(bf16[256,512]{1,0:T(8,128)(2,1)S(1)} %shard_map.96.refs_0_), channel_id=1, source_target_pairs={{0,1},{1,0},{2,3},{3,2},{4,5},{5,4},{6,7},{7,6},{8,9},{9,8},{10,11... | collective-permute-start | bytes 786440 | tf_op jit(solution)/shard_map/ppermute | solution.py:256
  68.3 16.5 %collective-permute-start.16 = (bf16[256,512]{1,0:T(8,128)(2,1)S(1)}, bf16[256,512]{1,0:T(8,128)(2,1)S(1)}, u32[]{:S(2)}, u32[]{:S(2)}) collective-permute-start(bf16[256,512]{1,0:T(8,128)(2,1)S(1)} %shard_map.98.refs_0_), channel_id=1, source_target_pairs={{0,2},{1,3},{2,0},{3,1},{4,6},{5,7},{6,4},{7,5},{8,10},{9,11},{10,... | collective-permute-start | bytes 786440 | tf_op jit(solution)/shard_map/ppermute | solution.py:256
  69.8 15.0 %collective-permute-start.5 = (bf16[256,512]{1,0:T(8,128)(2,1)S(1)}, bf16[256,512]{1,0:T(8,128)(2,1)}, u32[]{:S(2)}, u32[]{:S(2)}) collective-permute-start(bf16[256,512]{1,0:T(8,128)(2,1)S(1)} %collective-permute-done.4.refs_2_), channel_id=1, source_target_pairs={{0,1},{1,0},{2,3},{3,2},{4,5},{5,4},{6,7},{7,6},{8,9},{9,8},{10,11... | collective-permute-start | bytes 786440 | tf_op jit(solution)/shard_map/ppermute | solution.py:256
  74.1 13.3 %collective-permute-start.9 = (bf16[256,512]{1,0:T(8,128)(2,1)S(1)}, bf16[256,512]{1,0:T(8,128)(2,1)}, u32[]{:S(2)}, u32[]{:S(2)}) collective-permute-start(bf16[256,512]{1,0:T(8,128)(2,1)S(1)} %collective-permute-done.8.refs_2_), channel_id=1, source_target_pairs={{0,1},{1,0},{2,3},{3,2},{4,5},{5,4},{6,7},{7,6},{8,9},{9,8},{10,11... | collective-permute-start | bytes 786440 | tf_op jit(solution)/shard_map/ppermute | solution.py:256
  79.7 9.2 %collective-permute-start.13 = (bf16[256,512]{1,0:T(8,128)(2,1)S(1)}, bf16[256,512]{1,0:T(8,128)(2,1)S(1)}, u32[]{:S(2)}, u32[]{:S(2)}) collective-permute-start(bf16[256,512]{1,0:T(8,128)(2,1)S(1)} %collective-permute-done.12.refs_2_), channel_id=1, source_target_pairs={{0,1},{1,0},{2,3},{3,2},{4,5},{5,4},{6,7},{7,6},{8,9},{9,8},{10,11... | collective-permute-start | bytes 786440 | tf_op jit(solution)/shard_map/ppermute | solution.py:256
  79.7 9.7 %collective-permute-start.15 = (bf16[256,512]{1,0:T(8,128)(2,1)S(1)}, bf16[256,512]{1,0:T(8,128)(2,1)S(1)}, u32[]{:S(2)}, u32[]{:S(2)}) collective-permute-start(bf16[256,512]{1,0:T(8,128)(2,1)S(1)} %shard_map.98.refs_0_), channel_id=1, source_target_pairs={{0,1},{1,0},{2,3},{3,2},{4,5},{5,4},{6,7},{7,6},{8,9},{9,8},{10,11... | collective-permute-start | bytes 786440 | tf_op jit(solution)/shard_map/ppermute | solution.py:256
  80.9 19.9 %copy-start.6 = (bf16[256,512]{1,0:T(8,128)(2,1)S(1)}, bf16[256,512]{1,0:T(8,128)(2,1)}, u32[]{:S(2)}) copy-start(bf16[256,512]{1,0:T(8,128)(2,1)} %copy-done.5) | copy-start | bytes 786436
  84.8 7.5 %collective-permute-start.17 = (bf16[256,512]{1,0:T(8,128)(2,1)S(1)}, bf16[256,512]{1,0:T(8,128)(2,1)S(1)}, u32[]{:S(2)}, u32[]{:S(2)}) collective-permute-start(bf16[256,512]{1,0:T(8,128)(2,1)S(1)} %collective-permute-done.16.refs_2_), channel_id=1, source_target_pairs={{0,1},{1,0},{2,3},{3,2},{4,5},{5,4},{6,7},{7,6},{8,9},{9,8},{10,11... | collective-permute-start | bytes 786440 | tf_op jit(solution)/shard_map/ppermute | solution.py:256
  84.9 15.9 %collective-permute-start.37 = (bf16[256,512]{1,0:T(8,128)(2,1)}, bf16[256,512]{1,0:T(8,128)(2,1)S(1)}, u32[]{:S(2)}, u32[]{:S(2)}) collective-permute-start(bf16[256,512]{1,0:T(8,128)(2,1)} %get-tuple-element.63), channel_id=1, source_target_pairs={{0,12},{1,13},{2,14},{3,15},{4,8},{5,9},{6,10},{7,11},{8,4},{9,5},... | collective-permute-start | bytes 786440 | tf_op jit(solution)/shard_map/ppermute | solution.py:256
  87.4 15.0 %collective-permute-start.19 = (bf16[256,512]{1,0:T(8,128)(2,1)}, bf16[256,512]{1,0:T(8,128)(2,1)S(1)}, u32[]{:S(2)}, u32[]{:S(2)}) collective-permute-start(bf16[256,512]{1,0:T(8,128)(2,1)} %collective-permute-done.18.refs_5_), channel_id=1, source_target_pairs={{0,16},{1,17},{2,18},{3,19},{4,20},{5,21},{6,22},{7,23},{8,24},{9,... | collective-permute-start | bytes 786440 | tf_op jit(solution)/shard_map/ppermute | solution.py:256
  88.9 14.0 %collective-permute-start.21 = (bf16[256,512]{1,0:T(8,128)(2,1)}, bf16[256,512]{1,0:T(8,128)(2,1)S(1)}, u32[]{:S(2)}, u32[]{:S(2)}) collective-permute-start(bf16[256,512]{1,0:T(8,128)(2,1)} %collective-permute-done.20.refs_7_), channel_id=1, source_target_pairs={{0,16},{1,17},{2,18},{3,19},{4,20},{5,21},{6,22},{7,23},{8,24},{9,... | collective-permute-start | bytes 786440 | tf_op jit(solution)/shard_map/ppermute | solution.py:256
  89.4 3.6 %copy-start.1 = (bf16[256,512]{1,0:T(8,128)(2,1)}, bf16[256,512]{1,0:T(8,128)(2,1)S(1)}, u32[]{:S(2)}) copy-start(bf16[256,512]{1,0:T(8,128)(2,1)S(1)} %collective-permute-done.15.refs_1_) | copy-start | bytes 786436
  89.4 18.6 %collective-permute-start.23 = (bf16[256,512]{1,0:T(8,128)(2,1)}, bf16[256,512]{1,0:T(8,128)(2,1)S(1)}, u32[]{:S(2)}, u32[]{:S(2)}) collective-permute-start(bf16[256,512]{1,0:T(8,128)(2,1)} %collective-permute-done.22.refs_9_), channel_id=1, source_target_pairs={{0,16},{1,17},{2,18},{3,19},{4,20},{5,21},{6,22},{7,23},{8,24},{9,... | collective-permute-start | bytes 786440 | tf_op jit(solution)/shard_map/ppermute | solution.py:256
  92.3 21.3 %collective-permute-start.27 = (bf16[256,512]{1,0:T(8,128)(2,1)}, bf16[256,512]{1,0:T(8,128)(2,1)S(1)}, u32[]{:S(2)}, u32[]{:S(2)}) collective-permute-start(bf16[256,512]{1,0:T(8,128)(2,1)} %copy-done.7), channel_id=1, source_target_pairs={{0,16},{1,17},{2,18},{3,19},{4,20},{5,21},{6,22},{7,23},{8,24},{9,... | collective-permute-start | bytes 786440 | tf_op jit(solution)/shard_map/ppermute | solution.py:256
  98.2 0.9 copy-start.2
  100.8 18.4 %collective-permute-start.34 = (bf16[256,512]{1,0:T(8,128)(2,1)S(1)}, bf16[256,512]{1,0:T(8,128)(2,1)S(1)}, u32[]{:S(2)}, u32[]{:S(2)}) collective-permute-start(bf16[256,512]{1,0:T(8,128)(2,1)S(1)} %copy-done.6), channel_id=1, source_target_pairs={{0,16},{1,17},{2,18},{3,19},{4,20},{5,21},{6,22},{7,23},{8,24},{9,... | collective-permute-start | bytes 786440 | tf_op jit(solution)/shard_map/ppermute | solution.py:256
  102.3 21.8 %collective-permute-start.38 = (bf16[256,512]{1,0:T(8,128)(2,1)S(1)}, bf16[256,512]{1,0:T(8,128)(2,1)S(1)}, u32[]{:S(2)}, u32[]{:S(2)}) collective-permute-start(bf16[256,512]{1,0:T(8,128)(2,1)S(1)} %collective-permute-done.37.refs_0_), channel_id=1, source_target_pairs={{0,16},{1,17},{2,18},{3,19},{4,20},{5,21},{6,22},{7,23},{8,24},{9,... | collective-permute-start | bytes 786440 | tf_op jit(solution)/shard_map/ppermute | solution.py:256
  108.0 5.6 %copy-start.8 = (bf16[256,512]{1,0:T(8,128)(2,1)S(1)}, bf16[256,512]{1,0:T(8,128)(2,1)}, u32[]{:S(2)}) copy-start(bf16[256,512]{1,0:T(8,128)(2,1)} %copy-done.7) | copy-start | bytes 786436
  112.9 12.8 %collective-permute-start.24 = (bf16[512,512]{1,0:T(8,128)(2,1)S(1)}, bf16[512,512]{1,0:T(8,128)(2,1)S(1)}, u32[]{:S(2)}, u32[]{:S(2)}) collective-permute-start(bf16[512,512]{1,0:T(8,128)(2,1)S(1)} %get-tuple-element.40), channel_id=1, source_target_pairs={{0,1},{1,0},{2,3},{3,2},{4,5},{5,4},{6,7},{7,6},{8,9},{9,8},{10,11... | collective-permute-start | bytes 1572872 | tf_op jit(solution)/shard_map/ppermute | solution.py:256
  114.9 12.5 %collective-permute-start.28 = (bf16[512,512]{1,0:T(8,128)(2,1)S(1)}, bf16[512,512]{1,0:T(8,128)(2,1)S(1)}, u32[]{:S(2)}, u32[]{:S(2)}) collective-permute-start(bf16[512,512]{1,0:T(8,128)(2,1)S(1)} %get-tuple-element.44), channel_id=1, source_target_pairs={{0,1},{1,0},{2,3},{3,2},{4,5},{5,4},{6,7},{7,6},{8,9},{9,8},{10,11... | collective-permute-start | bytes 1572872 | tf_op jit(solution)/shard_map/ppermute | solution.py:256
  120.5 7.6 %collective-permute-start.35 = (bf16[512,512]{1,0:T(8,128)(2,1)S(1)}, bf16[512,512]{1,0:T(8,128)(2,1)S(1)}, u32[]{:S(2)}, u32[]{:S(2)}) collective-permute-start(bf16[512,512]{1,0:T(8,128)(2,1)S(1)} %get-tuple-element.52), channel_id=1, source_target_pairs={{0,1},{1,0},{2,3},{3,2},{4,5},{5,4},{6,7},{7,6},{8,9},{9,8},{10,11... | collective-permute-start | bytes 1572872 | tf_op jit(solution)/shard_map/ppermute | solution.py:256
  125.6 4.2 %collective-permute-start.39 = (bf16[512,512]{1,0:T(8,128)(2,1)S(1)}, bf16[512,512]{1,0:T(8,128)(2,1)S(1)}, u32[]{:S(2)}, u32[]{:S(2)}) collective-permute-start(bf16[512,512]{1,0:T(8,128)(2,1)S(1)} %get-tuple-element.56), channel_id=1, source_target_pairs={{0,1},{1,0},{2,3},{3,2},{4,5},{5,4},{6,7},{7,6},{8,9},{9,8},{10,11... | collective-permute-start | bytes 1572872 | tf_op jit(solution)/shard_map/ppermute | solution.py:256
  125.8 9.2 %collective-permute-start.25 = (bf16[256,512]{1,0:T(8,128)(2,1)S(1)}, bf16[256,512]{1,0:T(8,128)(2,1)S(1)}, u32[]{:S(2)}, u32[]{:S(2)}) collective-permute-start(bf16[256,512]{1,0:T(8,128)(2,1)S(1)} %get-tuple-element.42), channel_id=1, source_target_pairs={{0,2},{1,3},{2,0},{3,1},{4,6},{5,7},{6,4},{7,5},{8,10},{9,11},{10,... | collective-permute-start | bytes 786440 | tf_op jit(solution)/shard_map/ppermute | solution.py:256
  127.5 13.2 %collective-permute-start.29 = (bf16[256,512]{1,0:T(8,128)(2,1)S(1)}, bf16[256,512]{1,0:T(8,128)(2,1)S(1)}, u32[]{:S(2)}, u32[]{:S(2)}) collective-permute-start(bf16[256,512]{1,0:T(8,128)(2,1)S(1)} %get-tuple-element.46), channel_id=1, source_target_pairs={{0,2},{1,3},{2,0},{3,1},{4,6},{5,7},{6,4},{7,5},{8,10},{9,11},{10,... | collective-permute-start | bytes 786440 | tf_op jit(solution)/shard_map/ppermute | solution.py:256
  128.2 18.1 %collective-permute-start.36 = (bf16[256,512]{1,0:T(8,128)(2,1)S(1)}, bf16[256,512]{1,0:T(8,128)(2,1)S(1)}, u32[]{:S(2)}, u32[]{:S(2)}) collective-permute-start(bf16[256,512]{1,0:T(8,128)(2,1)S(1)} %get-tuple-element.54), channel_id=1, source_target_pairs={{0,2},{1,3},{2,0},{3,1},{4,6},{5,7},{6,4},{7,5},{8,10},{9,11},{10,... | collective-permute-start | bytes 786440 | tf_op jit(solution)/shard_map/ppermute | solution.py:256
  129.9 21.5 %collective-permute-start.40 = (bf16[256,512]{1,0:T(8,128)(2,1)S(1)}, bf16[256,512]{1,0:T(8,128)(2,1)S(1)}, u32[]{:S(2)}, u32[]{:S(2)}) collective-permute-start(bf16[256,512]{1,0:T(8,128)(2,1)S(1)} %get-tuple-element.58), channel_id=1, source_target_pairs={{0,2},{1,3},{2,0},{3,1},{4,6},{5,7},{6,4},{7,5},{8,10},{9,11},{10,... | collective-permute-start | bytes 786440 | tf_op jit(solution)/shard_map/ppermute | solution.py:256
  140.8 12.7 %collective-permute-start.30 = (bf16[64,1024]{1,0:T(8,128)(2,1)S(1)}, bf16[64,1024]{1,0:T(8,128)(2,1)S(1)}, u32[]{:S(2)}, u32[]{:S(2)}) collective-permute-start(bf16[64,1024]{1,0:T(8,128)(2,1)S(1)} %get-tuple-element.48), channel_id=1, source_target_pairs={{0,4},{1,5},{2,6},{3,7},{4,0},{5,1},{6,2},{7,3},{8,12},{9,13},{10,... | collective-permute-start | bytes 393224 | tf_op jit(solution)/shard_map/ppermute | solution.py:256
  140.9 15.1 %collective-permute-start.31 = (bf16[64,1024]{1,0:T(8,128)(2,1)S(1)}, bf16[64,1024]{1,0:T(8,128)(2,1)S(1)}, u32[]{:S(2)}, u32[]{:S(2)}) collective-permute-start(bf16[64,1024]{1,0:T(8,128)(2,1)S(1)} %get-tuple-element.49), channel_id=1, source_target_pairs={{0,8},{1,9},{2,10},{3,11},{4,12},{5,13},{6,14},{7,15},{8,0},{9,1},... | collective-permute-start | bytes 393224 | tf_op jit(solution)/shard_map/ppermute | solution.py:256
  142.8 13.2 %collective-permute-start.32 = (bf16[64,1024]{1,0:T(8,128)(2,1)S(1)}, bf16[64,1024]{1,0:T(8,128)(2,1)S(1)}, u32[]{:S(2)}, u32[]{:S(2)}) collective-permute-start(bf16[64,1024]{1,0:T(8,128)(2,1)S(1)} %get-tuple-element.50), channel_id=1, source_target_pairs={{0,12},{1,13},{2,14},{3,15},{4,8},{5,9},{6,10},{7,11},{8,4},{9,5},... | collective-permute-start | bytes 393224 | tf_op jit(solution)/shard_map/ppermute | solution.py:256
  151.5 6.8 %collective-permute-start.41 = (bf16[64,1024]{1,0:T(8,128)(2,1)S(1)}, bf16[64,1024]{1,0:T(8,128)(2,1)S(1)}, u32[]{:S(2)}, u32[]{:S(2)}) collective-permute-start(bf16[64,1024]{1,0:T(8,128)(2,1)S(1)} %get-tuple-element.60), channel_id=1, source_target_pairs={{0,4},{1,5},{2,6},{3,7},{4,0},{5,1},{6,2},{7,3},{8,12},{9,13},{10,... | collective-permute-start | bytes 393224 | tf_op jit(solution)/shard_map/ppermute | solution.py:256
  151.6 12.8 %collective-permute-start.42 = (bf16[64,1024]{1,0:T(8,128)(2,1)S(1)}, bf16[64,1024]{1,0:T(8,128)(2,1)S(1)}, u32[]{:S(2)}, u32[]{:S(2)}) collective-permute-start(bf16[64,1024]{1,0:T(8,128)(2,1)S(1)} %get-tuple-element.61), channel_id=1, source_target_pairs={{0,8},{1,9},{2,10},{3,11},{4,12},{5,13},{6,14},{7,15},{8,0},{9,1},... | collective-permute-start | bytes 393224 | tf_op jit(solution)/shard_map/ppermute | solution.py:256
  153.5 10.9 %collective-permute-start.43 = (bf16[64,1024]{1,0:T(8,128)(2,1)S(1)}, bf16[64,1024]{1,0:T(8,128)(2,1)S(1)}, u32[]{:S(2)}, u32[]{:S(2)}) collective-permute-start(bf16[64,1024]{1,0:T(8,128)(2,1)S(1)} %get-tuple-element.62), channel_id=1, source_target_pairs={{0,12},{1,13},{2,14},{3,15},{4,8},{5,9},{6,10},{7,11},{8,4},{9,5},... | collective-permute-start | bytes 393224 | tf_op jit(solution)/shard_map/ppermute | solution.py:256
  164.7 6.4 %collective-permute-start.45 = (bf16[64,2048]{1,0:T(8,128)(2,1)S(1)}, bf16[64,2048]{1,0:T(8,128)(2,1)S(1)}, u32[]{:S(2)}, u32[]{:S(2)}) collective-permute-start(bf16[64,2048]{1,0:T(8,128)(2,1)S(1)} %shard_map.111.refs_0_), channel_id=1, source_target_pairs={{0,2},{1,3},{2,0},{3,1},{4,6},{5,7},{6,4},{7,5},{8,10},{9,11},{10,... | collective-permute-start | bytes 786440 | tf_op jit(solution)/shard_map/ppermute | solution.py:256
  166.2 5.0 %collective-permute-start.44 = (bf16[64,2048]{1,0:T(8,128)(2,1)S(1)}, bf16[64,2048]{1,0:T(8,128)(2,1)S(1)}, u32[]{:S(2)}, u32[]{:S(2)}) collective-permute-start(bf16[64,2048]{1,0:T(8,128)(2,1)S(1)} %shard_map.111.refs_0_), channel_id=1, source_target_pairs={{0,1},{1,0},{2,3},{3,2},{4,5},{5,4},{6,7},{7,6},{8,9},{9,8},{10,11... | collective-permute-start | bytes 786440 | tf_op jit(solution)/shard_map/ppermute | solution.py:256
  171.1 1.5 collective-permute-start.46

commit v2 on v1

--- a/solution.py
+++ b/solution.py
@@ -104,7 +104,7 @@
         scratch_shapes=[pltpu.VMEM(shape, kind) for shape, kind in scratch],
         compiler_params=pltpu.CompilerParams(vmem_limit_bytes=min(3 * held + (8 << 20), 60 << 20)),
         cost_estimate=pl.CostEstimate(flops=max(flops, 1 << 20), bytes_accessed=moved, transcendentals=0),
-    )(jnp.stack([jnp.int32(v) for v in scalars]), *arrays)
+    )(scalars, *arrays)
 
 
 def array(shape, kind=jnp.bfloat16):
@@ -113,6 +113,13 @@
 
 def at(index, size):
     return pl.ds(pl.multiple_of(index * size, size), size)
+
+
+def rows_of(j, m):
+    place = 0
+    for bit in bits_of(m):
+        place = 2 * place + (j // bit) % 2
+    return place
 
 
 def prep_kernel(scalars, tokens, packed):
@@ -125,22 +132,37 @@
         piece = inverse.astype(jnp.bfloat16).astype(jnp.float32)
         pieces = jnp.where(lane == place, piece, pieces)
         inverse = inverse - piece
-    packed[:rows, :] = tokens[:, at(scalars[0], width)]
+    packed[:rows, :] = tokens[:, at(scalars[2], width)]
     packed[rows:, :] = jnp.zeros((packed.shape[0] - rows, width), jnp.bfloat16)
     packed[rows:, :rows] = jnp.transpose(pieces)[: packed.shape[0] - rows].astype(jnp.bfloat16)
 
 
+def columns_kernel(scalars, weight, own, *outs):
+    rows, units = outs[0].shape
+    own[...] = weight[:, at(scalars[1], units)].astype(jnp.bfloat16)
+    for d, out in enumerate(outs, 1):
+        out[...] = weight[at(scalars[0], rows), at(scalars[1] ^ d, units)].astype(jnp.bfloat16)
+
+
+def rows_kernel(scalars, weight, own, *outs):
+    rows, units = outs[0].shape[0], own.shape[0]
+    own[...] = weight[at(scalars[1], units), :].astype(jnp.bfloat16)
+    for d, out in enumerate(outs, 1):
+        part = (scalars[1] ^ d) * (units // rows) + scalars[0]
+        out[...] = weight[at(part, rows), :].astype(jnp.bfloat16)
+
+
 def mix_kernel(scalars, packed, gain, scale, *refs):
     *pieces, carried, mixer = refs
-    rows, depth = carried.shape[0], pieces[0].shape[0]
+    (rows, width), depth = carried.shape, pieces[0].shape[0]
     for d, piece in enumerate(pieces):
-        mixer[at(scalars[0] ^ d, depth), :] = piece[...]
+        mixer[at(scalars[1] ^ d, depth), :] = piece[...]
     tokens = packed[:rows, :].astype(jnp.float32)
     three = packed[rows:, :rows].astype(jnp.float32)
     inverse = three[0:1] + three[1:2] + three[2:3]
     inverse = jnp.transpose(jnp.broadcast_to(inverse, (128, rows)))[:, :1]
-    normed = (tokens * inverse * gain[...]).astype(jnp.bfloat16)
-    window = jnp.left_shift(jnp.int32(2), scalars[1])
+    normed = (tokens * inverse * gain[:, at(scalars[2], width)]).astype(jnp.bfloat16)
+    window = jnp.left_shift(jnp.int32(2), scalars[2])
     row = lax.broadcasted_iota(jnp.int32, (LENGTH, LENGTH), 0)
     offset = row - lax.broadcasted_iota(jnp.int32, (LENGTH, LENGTH), 1)
     band = jnp.where((offset >= 0) & (offset < window), 1.0, 0.0).astype(jnp.bfloat16)
@@ -154,56 +176,57 @@
         carried[here, :] = (tokens[here] + mixed).astype(jnp.bfloat16)
 
 
-def norm_kernel(scalars, gain, *refs):
-    *columns, normed, kept = refs
+def up_kernel(scalars, gain, scale, *refs, n, m, reps):
+    columns, pieces, (hidden, weight, values) = refs[: n * m], refs[n * m : -3], refs[-3:]
     rows, width = columns[0].shape
-    total = jnp.zeros((rows, 1), jnp.float32)
-    for column in columns:
-        value = column[...].astype(jnp.float32)
-        total = total + jnp.sum(value * value, axis=-1, keepdims=True)
-    inverse = lax.rsqrt(total / (width * len(columns)) + norm_eps)
-    for e, column in enumerate(columns):
-        place = at(scalars[0] ^ e, width)
-        value = column[...].astype(jnp.float32) * inverse * gain[:, place]
-        normed[:, place] = value.astype(jnp.bfloat16)
-        kept[:, place] = column[at(scalars[1], kept.shape[0]), :]
-
-
-def up_kernel(scalars, scale, *refs, n, reps):
-    normed, pieces, (hidden, weight) = refs[:n], refs[n:-2], refs[-2:]
-    rows = normed[0].shape[0]
-    own, pieces = pieces[0], pieces[1:]
-    depth = own.shape[0]
-    weight[at(scalars[0], depth), :] = own[...]
-    for place, piece in enumerate(pieces):
+    units = weight.shape[1]
+
+    def put(piece, block, part, parts):
+        size = width // parts
+        place = block * parts + part
+        tall = jnp.transpose(jnp.broadcast_to(gain[:, at(place, size)], (128, size)))[:, :1]
+        weight[at(place, size), :] = (piece[...].astype(jnp.float32) * tall).astype(jnp.bfloat16)
+
+    put(pieces[0], scalars[1], 0, 1)
+    for place, piece in enumerate(pieces[1:]):
         d, k = place // reps + 1, place % reps
-        part = lax.rem(scalars[1] - k + reps, reps)
-        weight[at((scalars[0] ^ d) * reps + part, depth // reps), :] = piece[...]
-    for d in range(n):
-        value = jnp.dot(normed[d][...], weight[...], preferred_element_type=jnp.float32)
-        value = jnp.maximum(value * scale[...], 0.0)
-        hidden[d * rows : (d + 1) * rows, :] = (value * value).astype(jnp.bfloat16)
-
-
-def down_kernel(scalars, hidden, scale, *refs, n):
+        put(piece, scalars[1] ^ d, lax.rem(scalars[0] - k + reps, reps), reps)
+    for b in range(n):
+        total = jnp.zeros((rows, 1), jnp.float32)
+        for e in range(m):
+            column = columns[b * m + e][...]
+            values[:, at(scalars[2] ^ e, width)] = column
+            column = column.astype(jnp.float32)
+            total = total + jnp.sum(column * column, axis=-1, keepdims=True)
+        inverse = lax.rsqrt(total / (width * m) + norm_eps)
+        own_scale = scale[:, at(scalars[1], units)]
+        value = jnp.dot(values[...], weight[...], preferred_element_type=jnp.float32)
+        value = jnp.maximum(value * inverse * own_scale, 0.0)
+        hidden[b * rows : (b + 1) * rows, :] = (value * value).astype(jnp.bfloat16)
+
+
+def down_kernel(scalars, hidden, scale, *refs, n, d):
     *pieces, stays, goes, weight = refs
     size = weight.shape[0] // len(pieces)
     for k, piece in enumerate(pieces):
         part = lax.rem(scalars[0] - k + len(pieces), len(pieces))
         weight[at(part, size), :] = piece[...]
-    half = stays.shape[0] // n
-    for b in range(n):
-        for out, side in ((goes, 1 - scalars[1]), (stays, scalars[1])):
+    half, cols = stays.shape[0] // n, stays.shape[1]
+    mine = scalars[2] % 2
+    own_scale = scale[:, at(scalars[1] ^ d, cols)]
+    for out, side in ((goes, 1 - mine), (stays, mine)):
+        for b in range(n):
             value = jnp.dot(
                 hidden[at(2 * b + side, half), :], weight[...], preferred_element_type=jnp.float32
             )
-            out[b * half : (b + 1) * half, :] = (value * scale[...]).astype(jnp.bfloat16)
-
-
-def fold_kernel(scalars, stayed, got, stays, goes, *, n):
+            out[b * half : (b + 1) * half, :] = (value * own_scale).astype(jnp.bfloat16)
+
+
+def fold_kernel(scalars, stayed, got, stays, goes, *, n, bit):
     half = stays.shape[0] // n
+    mine = (scalars[2] // bit) % 2
     for b in range(n):
-        for out, side in ((goes, 1 - scalars[0]), (stays, scalars[0])):
+        for out, side in ((goes, 1 - mine), (stays, mine)):
             place = at(2 * b + side, half)
             value = stayed[place, :].astype(jnp.float32) + got[place, :].astype(jnp.float32)
             out[b * half : (b + 1) * half, :] = value.astype(jnp.bfloat16)
@@ -221,24 +244,29 @@
             out[:, c * width : (c + 1) * width] = value.astype(jnp.bfloat16)
 
 
-def final_kernel(scalars, kept, *refs, n):
-    *sums, out = refs
-    width = out.shape[1] // n
-    groups = len(sums) // n
+def final_kernel(scalars, *refs, n, m, groups):
+    columns, terms, out = refs[:m], refs[m:-1], refs[-1]
+    rows, width = out.shape[0], columns[0].shape[1]
+    here = at(rows_of(scalars[2], m), rows)
     for q in range(n):
-        place = at(scalars[0] ^ q, width)
-        value = kept[:, place].astype(jnp.float32)
+        value = jnp.zeros((rows, width), jnp.float32)
         for e in range(n):
-            side, column = divmod(q ^ e, n // groups)
-            piece = sums[side * n + e][:, column * width : (column + 1) * width]
-            value = value + piece.astype(jnp.float32)
+            for g, group in enumerate(groups):
+                if q ^ e in group:
+                    place = group.index(q ^ e) * width
+                    piece = terms[g * n + e][:, place : place + width]
+                    value = value + piece.astype(jnp.float32)
+        out[:, at(scalars[1] ^ q, width)] = value.astype(jnp.bfloat16)
+    for e in range(m):
+        place = at(scalars[2] ^ e, width)
+        value = columns[e][here, :].astype(jnp.float32) + out[:, place].astype(jnp.float32)
         out[:, place] = value.astype(jnp.bfloat16)
 
 
-def place_kernel(scalars, *refs):
+def place_kernel(scalars, *refs, m):
     *parts, out = refs
     for e, part in enumerate(parts):
-        out[at(scalars[e], part.shape[0]), :] = part[...]
+        out[at(rows_of(scalars[2] ^ e, m), part.shape[0]), :] = part[...]
 
 
 def exchange_body(sizes):
@@ -268,12 +296,6 @@
             for e in list(held):
                 held[e ^ bit] = hop(held[e], tp=bit)
         return [held[e] for e in range(m)]
-
-    def rank_of_rows(j):
-        place = 0
-        for bit in tp_bits:
-            place = 2 * place + (j // bit) % 2
-        return place
 
     def body(
         tokens,
@@ -287,61 +309,51 @@
         down_scale,
     ):
         rows, model_width = tokens.shape
-        r, i, j = (lax.axis_index(axis) for axis in axes)
+        me = jnp.stack([lax.axis_index(axis) for axis in axes])
         width = group_weight.shape[1]
         units = up_weight.shape[1] // n
         cols = down_weight.shape[1]
+        part_rows = rows // m
 
         mixer = spread_fs(group_weight.astype(jnp.bfloat16))
-        (packed,) = local(prep_kernel, [array((rows + 16, width))], [j], tokens)
+        (packed,) = local(prep_kernel, [array((rows + 16, width))], me, tokens)
         blocks = spread_fs(packed)
 
-        def send_parts(block_of):
-            got = [[block_of(0).astype(jnp.bfloat16)]]
-            for d in range(1, n):
-                block = block_of(d)
-                part = block.shape[0] // reps
-                part = lax.dynamic_slice_in_dim(block, r * part, part, 0).astype(jnp.bfloat16)
-                part = hop(part, fs=d)
-                got.append([part] + [hop(part, rep=k) for k in range(1, reps)])
+        def send_parts(kernel, weight, own, part):
+            own, *outs = local(kernel, [array(own)] + [array(part)] * (n - 1), me, weight)
+            got = [own]
+            for d, out in enumerate(outs, 1):
+                out = hop(out, fs=d)
+                got.append(out)
+                got += [hop(out, rep=k) for k in range(1, reps)]
             return got
 
-        ups = send_parts(lambda d: lax.dynamic_slice_in_dim(up_weight, (i ^ d) * units, units, 1))
-        downs = send_parts(lambda d: lax.dynamic_slice_in_dim(down_weight, (i ^ d) * units, units, 0))
-
-        gain = lax.dynamic_slice_in_dim(mix_gain.reshape(1, -1), j * width, width, 1)
-        normed, kept = [], None
-        part_rows = rows // m
+        ups = send_parts(columns_kernel, up_weight, (width, units), (width // reps, units))
+        downs = send_parts(rows_kernel, down_weight, (units, cols), (units // reps, cols))
+
+        columns = []
         for d in range(n):
             (carried,) = local(
-                mix_kernel, [array((rows, width))], [i, j],
-                blocks[d], gain, group_scale, *mixer,
+                mix_kernel, [array((rows, width))], me,
+                blocks[d], mix_gain.reshape(1, -1), group_scale, *mixer,
                 scratch=[((n * group_weight.shape[0], width), jnp.bfloat16)],
                 flops=2 * rows * width * (width + LENGTH),
             )
-            columns = gather_tp(carried)
-            value, part = local(
-                norm_kernel, [array((rows, model_width)), array((part_rows, model_width))],
-                [j, rank_of_rows(j)], mlp_gain.reshape(1, -1), *columns,
-                flops=10 * rows * model_width,
-            )
-            normed.append(value)
-            kept = part if d == 0 else kept
+            columns += gather_tp(carried)
         (hidden,) = local(
-            functools.partial(up_kernel, n=n, reps=reps), [array((n * rows, units))], [i, r],
-            lax.dynamic_slice_in_dim(up_scale, i * units, units, 1),
-            *normed, *(p for block in ups for p in block),
-            scratch=[((model_width, units), jnp.bfloat16)],
+            functools.partial(up_kernel, n=n, m=m, reps=reps), [array((n * rows, units))], me,
+            mlp_gain.reshape(1, -1), up_scale, *columns, *ups,
+            scratch=[((model_width, units), jnp.bfloat16), ((rows, model_width), jnp.bfloat16)],
             flops=2 * n * rows * model_width * units,
         )
 
         sums = []
         for d in range(n):
-            scale = lax.dynamic_slice_in_dim(down_scale, (i ^ d) * cols, cols, 1)
             half = array((n * rows // 2, cols))
+            pieces = downs[:1] if d == 0 else downs[1 + (d - 1) * reps : 1 + d * reps]
             stays, goes = local(
-                functools.partial(down_kernel, n=n), [half, half], [r, j % 2],
-                hidden, scale, *downs[d],
+                functools.partial(down_kernel, n=n, d=d), [half, half], me,
+                hidden, down_scale, *pieces,
                 scratch=[((units, cols), jnp.bfloat16)],
                 flops=2 * n * rows * units * cols,
             )
@@ -349,26 +361,27 @@
                 got = hop(goes, tp=bit // 2)
                 half = array((half.shape[0] // 2, cols))
                 stays, goes = local(
-                    functools.partial(fold_kernel, n=n), [half, half],
-                    [(j // bit) % 2], stays, got,
+                    functools.partial(fold_kernel, n=n, bit=bit), [half, half],
+                    me, stays, got,
                 )
-            sums += [stays, hop(goes, tp=tp_bits[-1])]
+            sums.append((stays, hop(goes, tp=tp_bits[-1])))
+        groups = [[*range(n // 2)]] + [[d] for d in range(n // 2, n)]
         terms = []
-        for side in range(2):
-            mine = sums[side * n : (side + 1) * n]
+        for group in groups:
             outs = local(
                 functools.partial(sum_kernel, n=n),
-                [array((part_rows, cols * n // 2))] * n, [i], *mine,
+                [array((part_rows, cols * len(group)))] * n, me,
+                *(term for d in group for term in sums[d]),
             )
-            terms += [outs[0]] + [hop(outs[e], fs=e) for e in range(1, n)]
+            terms += [outs[0]]
+            terms += [hop(outs[e], fs=e) for e in range(1, n)]
         (out,) = local(
-            functools.partial(final_kernel, n=n), [array((part_rows, model_width))], [i],
-            kept, *terms,
-        )
-        parts = gather_tp(out)
+            functools.partial(final_kernel, n=n, m=m, groups=groups),
+            [array((part_rows, model_width))], me, *columns[:m], *terms,
+        )
         (out,) = local(
-            place_kernel, [array((rows, model_width))],
-            [rank_of_rows(j ^ e) for e in range(m)], *parts,
+            functools.partial(place_kernel, m=m), [array((rows, model_width))], me,
+            *gather_tp(out),
         )
         return out
 

time: 175 us -> 179 us (1.023)
  starting transfers between devices: 47.4 us -> 58.5 us
  local copies, waits for them, and re-layouts: 10.4 us -> 2.22 us
    ppermute x47 -> x50, starting transfers between devices: 47.4 us -> 58.5 us  [hop(): return lax.ppermute(values, axes, pairs)]
    convert_element_type x3 -> x0, local copies, waits for them, and re-layouts: 4.9 us -> none  [the longest x2 2.62 us: send_parts(): got = [[block_of(0).astype(jnp.bfloat16)]]]
    dynamic_slice x2 -> x0, local copies, waits for them, and re-layouts: 2.53 us -> none  [the longest x1 1.84 us: send_parts(): lax.dynamic_slice_in_dim(block, r * part, part, 0).astype(jnp.bfloat16)]
    ppermute x47 -> x50, waiting for transfers between devices: 91 us -> 91.9 us  [hop(): return lax.ppermute(values, axes, pairs)]
    pallas_call x22 -> x21, Pallas kernels: 23.9 us -> 23.8 us  [local(): pl.pallas_call(kernel, out_shape=outs, in_specs=[pl.BlockSpec(memory_spac...]
  transfers between devices with their start and end apart: 47 -> 50, of which waited for: 19 -> 15; matrix products, arithmetic and copies ran while one was open for 5% -> 0% of each run, Pallas kernels for 13% -> 12%
where the time goes in v2:
time: 179 us; the launch traced here: 178 us
  waiting for transfers between devices  91.9 us (51%)
  starting transfers between devices  58.5 us (33%)
  Pallas kernels  23.8 us (13%)
  local copies, waits for them, and re-layouts  2.22 us (1%)
    ppermute x50, waiting for transfers between devices, hop(): return lax.ppermute(values, axes, pairs)  91.9 us
    ppermute x50, starting transfers between devices, hop(): return lax.ppermute(values, axes, pairs)  58.5 us
    pallas_call x21, Pallas kernels, local(): pl.pallas_call(kernel, out_shape=outs, in_specs=[pl.BlockSpec(memory_spac...  23.8 us
  transfers between devices with their start and end apart: 50, of which 15 were waited for; matrix products, arithmetic and copies ran while one was open for 0% of the time, Pallas kernels for 12%

profile of v2, /device:TPU:0, one launch (start us, length us, event | category | flops | bytes accessed | tf_op | source)
XLA Modules:
  0.0 177.8 jit_solution(4631133070423515307)
XLA Ops:
  0.0 1.0 convert_element_type.3.refs_0_
  1.0 4.1 %collective-permute-start.1 = (bf16[128,512]{1,0:T(8,128)(2,1)S(1)}, bf16[128,512]{1,0:T(8,128)(2,1)S(1)}, u32[]{:S(2)}, u32[]{:S(2)}) collective-permute-start(bf16[128,512]{1,0:T(8,128)(2,1)S(1)} %convert_element_type.3.refs_0_), channel_id=1, source_target_pairs={{0,8},{1,9},{2,10},{3,11},{4,12},{5,13},{6,14},{7,15},{8,0},{9,1},... | collective-permute-start | bytes 393224 | tf_op jit(solution)/shard_map/ppermute | solution.py:284
  5.1 1.6 collective-permute-start
  6.8 2.2 %copy-done = f32[512,2048]{1,0:T(8,128)S(1)} copy-done((f32[512,2048]{1,0:T(8,128)S(1)}, f32[512,2048]{1,0:T(8,128)}, u32[]{:S(2)}) %copy-start) | copy-done | bytes 4194328
  9.0 0.7 shard_map.96
  10.2 3.9 %collective-permute-start.22 = (bf16[256,512]{1,0:T(8,128)(2,1)S(1)}, bf16[256,512]{1,0:T(8,128)(2,1)S(1)}, u32[]{:S(2)}, u32[]{:S(2)}) collective-permute-start(bf16[256,512]{1,0:T(8,128)(2,1)S(1)} %get-tuple-element.44), channel_id=1, source_target_pairs={{0,12},{1,13},{2,14},{3,15},{4,8},{5,9},{6,10},{7,11},{8,4},{9,5},... | collective-permute-start | bytes 786440 | tf_op jit(solution)/shard_map/ppermute | solution.py:284
  14.1 0.7 shard_map.98
  14.9 2.0 %collective-permute-start.2 = (bf16[128,512]{1,0:T(8,128)(2,1)S(1)}, bf16[128,512]{1,0:T(8,128)(2,1)S(1)}, u32[]{:S(2)}, u32[]{:S(2)}) collective-permute-start(bf16[128,512]{1,0:T(8,128)(2,1)S(1)} %collective-permute-done.1.refs_2_), channel_id=1, source_target_pairs={{0,4},{1,5},{2,6},{3,7},{4,0},{5,1},{6,2},{7,3},{8,12},{9,13},{10,... | collective-permute-start | bytes 393224 | tf_op jit(solution)/shard_map/ppermute | solution.py:284
  16.9 0.9 shard_map.91.packed
  17.8 19.2 %collective-permute-done.2.refs_3_ = bf16[128,512]{1,0:T(8,128)(2,1)S(1)} collective-permute-done((bf16[128,512]{1,0:T(8,128)(2,1)S(1)}, bf16[128,512]{1,0:T(8,128)(2,1)S(1)}, u32[]{:S(2)}, u32[]{:S(2)}) %collective-permute-start.2) | collective-permute-done | bytes 131104 | tf_op jit(solution)/shard_map/ppermute | solution.py:284
  37.0 1.5 collective-permute-start.10
  38.5 1.6 collective-permute-start.6
  40.1 1.4 collective-permute-start.33
  41.5 1.4 collective-permute-start.40
  42.9 1.3 shard_map.92.refs_0_
  44.2 1.6 collective-permute-start.4
  45.7 8.8 %collective-permute-done.10.packed = bf16[272,512]{1,0:T(8,128)(2,1)S(1)} collective-permute-done((bf16[272,512]{1,0:T(8,128)(2,1)S(1)}, bf16[272,512]{1,0:T(8,128)(2,1)S(1)}, u32[]{:S(2)}, u32[]{:S(2)}) %collective-permute-start.10) | collective-permute-done | bytes 278560 | tf_op jit(solution)/shard_map/ppermute | solution.py:284
  54.5 14.8 %collective-permute-done.33.refs_0_ = bf16[256,512]{1,0:T(8,128)(2,1)S(1)} collective-permute-done((bf16[256,512]{1,0:T(8,128)(2,1)S(1)}, bf16[256,512]{1,0:T(8,128)(2,1)S(1)}, u32[]{:S(2)}, u32[]{:S(2)}) %collective-permute-start.33) | collective-permute-done | bytes 262176 | tf_op jit(solution)/shard_map/ppermute | solution.py:284
  69.4 1.5 collective-permute-start.19
  71.4 1.5 collective-permute-start.23
  72.9 1.3 shard_map.94.refs_8_
  74.2 1.6 collective-permute-start.12
  75.8 1.3 shard_map.93.refs_4_
  77.1 1.3 shard_map.95.refs_12_
  78.6 1.5 collective-permute-start.8
  80.0 4.1 %collective-permute-done.21.refs_20_ = bf16[256,512]{1,0:T(8,128)(2,1)S(1)} collective-permute-done((bf16[256,512]{1,0:T(8,128)(2,1)S(1)}, bf16[256,512]{1,0:T(8,128)(2,1)S(1)}, u32[]{:S(2)}, u32[]{:S(2)}) %collective-permute-start.21) | collective-permute-done | bytes 262176 | tf_op jit(solution)/shard_map/ppermute | solution.py:284
  84.2 5.2 %collective-permute-done.23.refs_22_ = bf16[256,512]{1,0:T(8,128)(2,1)S(1)} collective-permute-done((bf16[256,512]{1,0:T(8,128)(2,1)S(1)}, bf16[256,512]{1,0:T(8,128)(2,1)S(1)}, u32[]{:S(2)}, u32[]{:S(2)}) %collective-permute-start.23) | collective-permute-done | bytes 262176 | tf_op jit(solution)/shard_map/ppermute | solution.py:284
  89.3 1.5 collective-permute-start.16
  91.9 5.3 %collective-permute-done.16.refs_14_ = bf16[256,512]{1,0:T(8,128)(2,1)S(1)} collective-permute-done((bf16[256,512]{1,0:T(8,128)(2,1)S(1)}, bf16[256,512]{1,0:T(8,128)(2,1)S(1)}, u32[]{:S(2)}, u32[]{:S(2)}) %collective-permute-start.16) | collective-permute-done | bytes 262176 | tf_op jit(solution)/shard_map/ppermute | solution.py:284
  97.2 1.5 collective-permute-start.34
  99.2 1.5 collective-permute-start.41
  100.8 4.3 %shard_map.97.hidden = bf16[1024,512]{1,0:T(8,128)(2,1)S(1)} custom-call(s32[3]{0:T(128)S(1)} %pad_add_fusion.scalars, f32[1,2048]{1,0:T(1,128)S(1)} %bitcast.9, f32[1,2048]{1,0:T(1,128)S(1)} %copy-done.6, bf16[256,512]{1,0:T(8,128)(2,1)S(1)} %shard_map.92.refs_0_, bf16[256,512]{1,0:T(8,128)(2,1)S(1)} %collective-permute-done.3.refs_1_, ...), custom_call_target="tpu_custom_call" | custom-call | flops 2147483648 | bytes 7356416 | tf_op jit(solution)/shard_map/pallas_call | solution.py:98
  105.1 1.3 collective-permute-done.34.refs_1_
  106.4 1.3 shard_map.104
  107.8 1.3 shard_map.99
  109.1 2.9 %collective-permute-done.27.refs_1_ = bf16[256,512]{1,0:T(8,128)(2,1)S(1)} collective-permute-done((bf16[256,512]{1,0:T(8,128)(2,1)S(1)}, bf16[256,512]{1,0:T(8,128)(2,1)S(1)}, u32[]{:S(2)}, u32[]{:S(2)}) %collective-permute-start.27) | collective-permute-done | bytes 262176 | tf_op jit(solution)/shard_map/ppermute | solution.py:284
  112.0 1.3 shard_map.101
  113.9 3.3 %collective-permute-done.41.refs_1_ = bf16[256,512]{1,0:T(8,128)(2,1)S(1)} collective-permute-done((bf16[256,512]{1,0:T(8,128)(2,1)S(1)}, bf16[256,512]{1,0:T(8,128)(2,1)S(1)}, u32[]{:S(2)}, u32[]{:S(2)}) %collective-permute-start.41) | collective-permute-done | bytes 262176 | tf_op jit(solution)/shard_map/ppermute | solution.py:284
  117.2 1.3 shard_map.107
  118.6 0.7 shard_map.105
  119.2 1.6 collective-permute-start.36
  120.8 0.7 shard_map.102
  122.1 0.7 shard_map.100
  122.8 1.6 collective-permute-start.25
  124.3 0.7 shard_map.108
  125.6 2.9 %collective-permute-done.36.refs_1_ = bf16[256,512]{1,0:T(8,128)(2,1)S(1)} collective-permute-done((bf16[256,512]{1,0:T(8,128)(2,1)S(1)}, bf16[256,512]{1,0:T(8,128)(2,1)S(1)}, u32[]{:S(2)}, u32[]{:S(2)}) %collective-permute-start.36) | collective-permute-done | bytes 262176 | tf_op jit(solution)/shard_map/ppermute | solution.py:284
  128.5 0.6 shard_map.106
  129.1 2.7 %collective-permute-start.37 = (bf16[64,512]{1,0:T(8,128)(2,1)S(1)}, bf16[64,512]{1,0:T(8,128)(2,1)S(1)}, u32[]{:S(2)}, u32[]{:S(2)}) collective-permute-start(bf16[64,512]{1,0:T(8,128)(2,1)S(1)} %get-tuple-element.65), channel_id=1, source_target_pairs={{0,4},{1,5},{2,6},{3,7},{4,0},{5,1},{6,2},{7,3},{8,12},{9,13},{10,... | collective-permute-start | bytes 196616 | tf_op jit(solution)/shard_map/ppermute | solution.py:284
  131.8 2.6 %collective-permute-start.38 = (bf16[64,512]{1,0:T(8,128)(2,1)S(1)}, bf16[64,512]{1,0:T(8,128)(2,1)S(1)}, u32[]{:S(2)}, u32[]{:S(2)}) collective-permute-start(bf16[64,512]{1,0:T(8,128)(2,1)S(1)} %get-tuple-element.66), channel_id=1, source_target_pairs={{0,8},{1,9},{2,10},{3,11},{4,12},{5,13},{6,14},{7,15},{8,0},{9,1},... | collective-permute-start | bytes 196616 | tf_op jit(solution)/shard_map/ppermute | solution.py:284
  134.4 5.4 %collective-permute-done.25.refs_1_ = bf16[256,512]{1,0:T(8,128)(2,1)S(1)} collective-permute-done((bf16[256,512]{1,0:T(8,128)(2,1)S(1)}, bf16[256,512]{1,0:T(8,128)(2,1)S(1)}, u32[]{:S(2)}, u32[]{:S(2)}) %collective-permute-start.25) | collective-permute-done | bytes 262176 | tf_op jit(solution)/shard_map/ppermute | solution.py:284
  139.7 0.7 shard_map.103
  140.4 2.7 %collective-permute-start.30 = (bf16[64,1024]{1,0:T(8,128)(2,1)S(1)}, bf16[64,1024]{1,0:T(8,128)(2,1)S(1)}, u32[]{:S(2)}, u32[]{:S(2)}) collective-permute-start(bf16[64,1024]{1,0:T(8,128)(2,1)S(1)} %get-tuple-element.56), channel_id=1, source_target_pairs={{0,4},{1,5},{2,6},{3,7},{4,0},{5,1},{6,2},{7,3},{8,12},{9,13},{10,... | collective-permute-start | bytes 393224 | tf_op jit(solution)/shard_map/ppermute | solution.py:284
  143.0 4.0 %collective-permute-start.39 = (bf16[64,512]{1,0:T(8,128)(2,1)S(1)}, bf16[64,512]{1,0:T(8,128)(2,1)S(1)}, u32[]{:S(2)}, u32[]{:S(2)}) collective-permute-start(bf16[64,512]{1,0:T(8,128)(2,1)S(1)} %get-tuple-element.67), channel_id=1, source_target_pairs={{0,12},{1,13},{2,14},{3,15},{4,8},{5,9},{6,10},{7,11},{8,4},{9,5},... | collective-permute-start | bytes 196616 | tf_op jit(solution)/shard_map/ppermute | solution.py:284
  147.0 0.6 shard_map.109
  148.1 2.6 %collective-permute-start.31 = (bf16[64,1024]{1,0:T(8,128)(2,1)S(1)}, bf16[64,1024]{1,0:T(8,128)(2,1)S(1)}, u32[]{:S(2)}, u32[]{:S(2)}) collective-permute-start(bf16[64,1024]{1,0:T(8,128)(2,1)S(1)} %get-tuple-element.57), channel_id=1, source_target_pairs={{0,8},{1,9},{2,10},{3,11},{4,12},{5,13},{6,14},{7,15},{8,0},{9,1},... | collective-permute-start | bytes 393224 | tf_op jit(solution)/shard_map/ppermute | solution.py:284
  150.7 1.4 collective-permute-start.32
  152.2 2.0 %collective-permute-start.45 = (bf16[64,512]{1,0:T(8,128)(2,1)S(1)}, bf16[64,512]{1,0:T(8,128)(2,1)S(1)}, u32[]{:S(2)}, u32[]{:S(2)}) collective-permute-start(bf16[64,512]{1,0:T(8,128)(2,1)S(1)} %get-tuple-element.75), channel_id=1, source_target_pairs={{0,8},{1,9},{2,10},{3,11},{4,12},{5,13},{6,14},{7,15},{8,0},{9,1},... | collective-permute-start | bytes 196616 | tf_op jit(solution)/shard_map/ppermute | solution.py:284
  154.2 1.0 collective-permute-start.46
  155.1 12.3 %collective-permute-done.45.refs_14_ = bf16[64,512]{1,0:T(8,128)(2,1)S(1)} collective-permute-done((bf16[64,512]{1,0:T(8,128)(2,1)S(1)}, bf16[64,512]{1,0:T(8,128)(2,1)S(1)}, u32[]{:S(2)}, u32[]{:S(2)}) %collective-permute-start.45) | collective-permute-done | bytes 65568 | tf_op jit(solution)/shard_map/ppermute | solution.py:284
  167.4 0.8 shard_map.110.refs_0_
  168.2 1.7 collective-permute-start.48
  169.9 4.7 %collective-permute-done.48.refs_2_ = bf16[64,2048]{1,0:T(8,128)(2,1)S(1)} collective-permute-done((bf16[64,2048]{1,0:T(8,128)(2,1)S(1)}, bf16[64,2048]{1,0:T(8,128)(2,1)S(1)}, u32[]{:S(2)}, u32[]{:S(2)}) %collective-permute-start.48) | collective-permute-done | bytes 262176 | tf_op jit(solution)/shard_map/ppermute | solution.py:284
  174.6 1.5 collective-permute-done.49.refs_3_
  176.2 1.6 shard_map.111
  (75 shorter events, 5.4 us)
Async XLA Ops:
  1.0 13.8 %collective-permute-start.1 = (bf16[128,512]{1,0:T(8,128)(2,1)S(1)}, bf16[128,512]{1,0:T(8,128)(2,1)S(1)}, u32[]{:S(2)}, u32[]{:S(2)}) collective-permute-start(bf16[128,512]{1,0:T(8,128)(2,1)S(1)} %convert_element_type.3.refs_0_), channel_id=1, source_target_pairs={{0,8},{1,9},{2,10},{3,11},{4,12},{5,13},{6,14},{7,15},{8,0},{9,1},... | collective-permute-start | bytes 393224 | tf_op jit(solution)/shard_map/ppermute | solution.py:284
  5.1 9.8 %collective-permute-start = (bf16[128,512]{1,0:T(8,128)(2,1)S(1)}, bf16[128,512]{1,0:T(8,128)(2,1)S(1)}, u32[]{:S(2)}, u32[]{:S(2)}) collective-permute-start(bf16[128,512]{1,0:T(8,128)(2,1)S(1)} %convert_element_type.3.refs_0_), channel_id=1, source_target_pairs={{0,4},{1,5},{2,6},{3,7},{4,0},{5,1},{6,2},{7,3},{8,12},{9,13},{10,... | collective-permute-start | bytes 393224 | tf_op jit(solution)/shard_map/ppermute | solution.py:284
  6.8 2.2 %copy-start = (f32[512,2048]{1,0:T(8,128)S(1)}, f32[512,2048]{1,0:T(8,128)}, u32[]{:S(2)}) copy-start(f32[512,2048]{1,0:T(8,128)} %weight.2) | copy-start | bytes 12582916
  8.9 5.2 %copy-start.1 = (f32[2048,512]{1,0:T(8,128)S(1)}, f32[2048,512]{1,0:T(8,128)}, u32[]{:S(2)}) copy-start(f32[2048,512]{1,0:T(8,128)} %weight.3) | copy-start | bytes 12582916
  8.9 7.9 %copy-start.2 = (bf16[256,2048]{1,0:T(8,128)(2,1)S(1)}, bf16[256,2048]{1,0:T(8,128)(2,1)}, u32[]{:S(2)}) copy-start(bf16[256,2048]{1,0:T(8,128)(2,1)} %tokens.1) | copy-start | bytes 3145732
  8.9 33.9 %copy-start.3 = (f32[2048]{0:T(1024)S(1)}, f32[2048]{0:T(1024)}, u32[]{:S(2)}) copy-start(f32[2048]{0:T(1024)} %param.10) | copy-start | bytes 24580
  9.0 33.9 %copy-start.4 = (f32[1,512]{1,0:T(1,128)S(1)}, f32[1,512]{1,0:T(1,128)}, u32[]{:S(2)}) copy-start(f32[1,512]{1,0:T(1,128)} %scale.12) | copy-start | bytes 6148
  9.6 28.8 %collective-permute-start.18 = (bf16[256,512]{1,0:T(8,128)(2,1)S(1)}, bf16[256,512]{1,0:T(8,128)(2,1)S(1)}, u32[]{:S(2)}, u32[]{:S(2)}) collective-permute-start(bf16[256,512]{1,0:T(8,128)(2,1)S(1)} %get-tuple-element.42), channel_id=1, source_target_pairs={{0,4},{1,5},{2,6},{3,7},{4,0},{5,1},{6,2},{7,3},{8,12},{9,13},{10,... | collective-permute-start | bytes 786440 | tf_op jit(solution)/shard_map/ppermute | solution.py:284
  10.2 29.9 %collective-permute-start.20 = (bf16[256,512]{1,0:T(8,128)(2,1)S(1)}, bf16[256,512]{1,0:T(8,128)(2,1)S(1)}, u32[]{:S(2)}, u32[]{:S(2)}) collective-permute-start(bf16[256,512]{1,0:T(8,128)(2,1)S(1)} %get-tuple-element.43), channel_id=1, source_target_pairs={{0,8},{1,9},{2,10},{3,11},{4,12},{5,13},{6,14},{7,15},{8,0},{9,1},... | collective-permute-start | bytes 786440 | tf_op jit(solution)/shard_map/ppermute | solution.py:284
  10.2 90.5 %copy-start.5 = (f32[2048]{0:T(1024)S(1)}, f32[2048]{0:T(1024)}, u32[]{:S(2)}) copy-start(f32[2048]{0:T(1024)} %param.13) | copy-start | bytes 24580
  10.2 90.5 %copy-start.6 = (f32[1,2048]{1,0:T(1,128)S(1)}, f32[1,2048]{1,0:T(1,128)}, u32[]{:S(2)}) copy-start(f32[1,2048]{1,0:T(1,128)} %scale.13) | copy-start | bytes 24580
  10.2 31.2 %collective-permute-start.22 = (bf16[256,512]{1,0:T(8,128)(2,1)S(1)}, bf16[256,512]{1,0:T(8,128)(2,1)S(1)}, u32[]{:S(2)}, u32[]{:S(2)}) collective-permute-start(bf16[256,512]{1,0:T(8,128)(2,1)S(1)} %get-tuple-element.44), channel_id=1, source_target_pairs={{0,12},{1,13},{2,14},{3,15},{4,8},{5,9},{6,10},{7,11},{8,4},{9,5},... | collective-permute-start | bytes 786440 | tf_op jit(solution)/shard_map/ppermute | solution.py:284
  14.8 29.4 %collective-permute-start.26 = (bf16[256,512]{1,0:T(8,128)(2,1)S(1)}, bf16[256,512]{1,0:T(8,128)(2,1)S(1)}, u32[]{:S(2)}, u32[]{:S(2)}) collective-permute-start(bf16[256,512]{1,0:T(8,128)(2,1)S(1)} %get-tuple-element.50), channel_id=1, source_target_pairs={{0,4},{1,5},{2,6},{3,7},{4,0},{5,1},{6,2},{7,3},{8,12},{9,13},{10,... | collective-permute-start | bytes 786440 | tf_op jit(solution)/shard_map/ppermute | solution.py:284
  14.9 22.1 %collective-permute-start.2 = (bf16[128,512]{1,0:T(8,128)(2,1)S(1)}, bf16[128,512]{1,0:T(8,128)(2,1)S(1)}, u32[]{:S(2)}, u32[]{:S(2)}) collective-permute-start(bf16[128,512]{1,0:T(8,128)(2,1)S(1)} %collective-permute-done.1.refs_2_), channel_id=1, source_target_pairs={{0,4},{1,5},{2,6},{3,7},{4,0},{5,1},{6,2},{7,3},{8,12},{9,13},{10,... | collective-permute-start | bytes 393224 | tf_op jit(solution)/shard_map/ppermute | solution.py:284
  37.0 17.5 %collective-permute-start.10 = (bf16[272,512]{1,0:T(8,128)(2,1)S(1)}, bf16[272,512]{1,0:T(8,128)(2,1)S(1)}, u32[]{:S(2)}, u32[]{:S(2)}) collective-permute-start(bf16[272,512]{1,0:T(8,128)(2,1)S(1)} %shard_map.91.packed), channel_id=1, source_target_pairs={{0,8},{1,9},{2,10},{3,11},{4,12},{5,13},{6,14},{7,15},{8,0},{9,1},... | collective-permute-start | bytes 835592 | tf_op jit(solution)/shard_map/ppermute | solution.py:284
  38.5 32.4 %collective-permute-start.6 = (bf16[272,512]{1,0:T(8,128)(2,1)S(1)}, bf16[272,512]{1,0:T(8,128)(2,1)S(1)}, u32[]{:S(2)}, u32[]{:S(2)}) collective-permute-start(bf16[272,512]{1,0:T(8,128)(2,1)S(1)} %shard_map.91.packed), channel_id=1, source_target_pairs={{0,4},{1,5},{2,6},{3,7},{4,0},{5,1},{6,2},{7,3},{8,12},{9,13},{10,... | collective-permute-start | bytes 835592 | tf_op jit(solution)/shard_map/ppermute | solution.py:284
  40.1 29.3 %collective-permute-start.33 = (bf16[256,512]{1,0:T(8,128)(2,1)S(1)}, bf16[256,512]{1,0:T(8,128)(2,1)S(1)}, u32[]{:S(2)}, u32[]{:S(2)}) collective-permute-start(bf16[256,512]{1,0:T(8,128)(2,1)S(1)} %get-tuple-element.59), channel_id=1, source_target_pairs={{0,8},{1,9},{2,10},{3,11},{4,12},{5,13},{6,14},{7,15},{8,0},{9,1},... | collective-permute-start | bytes 786440 | tf_op jit(solution)/shard_map/ppermute | solution.py:284
  41.5 27.9 %collective-permute-start.40 = (bf16[256,512]{1,0:T(8,128)(2,1)S(1)}, bf16[256,512]{1,0:T(8,128)(2,1)S(1)}, u32[]{:S(2)}, u32[]{:S(2)}) collective-permute-start(bf16[256,512]{1,0:T(8,128)(2,1)S(1)} %get-tuple-element.68), channel_id=1, source_target_pairs={{0,12},{1,13},{2,14},{3,15},{4,8},{5,9},{6,10},{7,11},{8,4},{9,5},... | collective-permute-start | bytes 786440 | tf_op jit(solution)/shard_map/ppermute | solution.py:284
  44.2 27.2 %collective-permute-start.4 = (bf16[256,512]{1,0:T(8,128)(2,1)S(1)}, bf16[256,512]{1,0:T(8,128)(2,1)S(1)}, u32[]{:S(2)}, u32[]{:S(2)}) collective-permute-start(bf16[256,512]{1,0:T(8,128)(2,1)S(1)} %shard_map.92.refs_0_), channel_id=1, source_target_pairs={{0,2},{1,3},{2,0},{3,1},{4,6},{5,7},{6,4},{7,5},{8,10},{9,11},{10,... | collective-permute-start | bytes 786440 | tf_op jit(solution)/shard_map/ppermute | solution.py:284
  54.5 19.7 %collective-permute-start.14 = (bf16[272,512]{1,0:T(8,128)(2,1)S(1)}, bf16[272,512]{1,0:T(8,128)(2,1)S(1)}, u32[]{:S(2)}, u32[]{:S(2)}) collective-permute-start(bf16[272,512]{1,0:T(8,128)(2,1)S(1)} %collective-permute-done.10.packed), channel_id=1, source_target_pairs={{0,4},{1,5},{2,6},{3,7},{4,0},{5,1},{6,2},{7,3},{8,12},{9,13},{10,... | collective-permute-start | bytes 835592 | tf_op jit(solution)/shard_map/ppermute | solution.py:284
  69.4 9.0 %collective-permute-start.3 = (bf16[256,512]{1,0:T(8,128)(2,1)S(1)}, bf16[256,512]{1,0:T(8,128)(2,1)S(1)}, u32[]{:S(2)}, u32[]{:S(2)}) collective-permute-start(bf16[256,512]{1,0:T(8,128)(2,1)S(1)} %shard_map.92.refs_0_), channel_id=1, source_target_pairs={{0,1},{1,0},{2,3},{3,2},{4,5},{5,4},{6,7},{7,6},{8,9},{9,8},{10,11... | collective-permute-start | bytes 786440 | tf_op jit(solution)/shard_map/ppermute | solution.py:284
  69.4 9.2 %collective-permute-start.19 = (bf16[256,512]{1,0:T(8,128)(2,1)S(1)}, bf16[256,512]{1,0:T(8,128)(2,1)S(1)}, u32[]{:S(2)}, u32[]{:S(2)}) collective-permute-start(bf16[256,512]{1,0:T(8,128)(2,1)S(1)} %collective-permute-done.18.refs_17_), channel_id=1, source_target_pairs={{0,16},{1,17},{2,18},{3,19},{4,20},{5,21},{6,22},{7,23},{8,24},{9,... | collective-permute-start | bytes 786440 | tf_op jit(solution)/shard_map/ppermute | solution.py:284
  70.9 13.3 %collective-permute-start.21 = (bf16[256,512]{1,0:T(8,128)(2,1)S(1)}, bf16[256,512]{1,0:T(8,128)(2,1)S(1)}, u32[]{:S(2)}, u32[]{:S(2)}) collective-permute-start(bf16[256,512]{1,0:T(8,128)(2,1)S(1)} %collective-permute-done.20.refs_19_), channel_id=1, source_target_pairs={{0,16},{1,17},{2,18},{3,19},{4,20},{5,21},{6,22},{7,23},{8,24},{9,... | collective-permute-start | bytes 786440 | tf_op jit(solution)/shard_map/ppermute | solution.py:284
  71.4 17.9 %collective-permute-start.23 = (bf16[256,512]{1,0:T(8,128)(2,1)S(1)}, bf16[256,512]{1,0:T(8,128)(2,1)S(1)}, u32[]{:S(2)}, u32[]{:S(2)}) collective-permute-start(bf16[256,512]{1,0:T(8,128)(2,1)S(1)} %collective-permute-done.22.refs_21_), channel_id=1, source_target_pairs={{0,16},{1,17},{2,18},{3,19},{4,20},{5,21},{6,22},{7,23},{8,24},{9,... | collective-permute-start | bytes 786440 | tf_op jit(solution)/shard_map/ppermute | solution.py:284
  74.2 16.6 %collective-permute-start.12 = (bf16[256,512]{1,0:T(8,128)(2,1)S(1)}, bf16[256,512]{1,0:T(8,128)(2,1)S(1)}, u32[]{:S(2)}, u32[]{:S(2)}) collective-permute-start(bf16[256,512]{1,0:T(8,128)(2,1)S(1)} %shard_map.94.refs_8_), channel_id=1, source_target_pairs={{0,2},{1,3},{2,0},{3,1},{4,6},{5,7},{6,4},{7,5},{8,10},{9,11},{10,... | collective-permute-start | bytes 786440 | tf_op jit(solution)/shard_map/ppermute | solution.py:284
  78.4 28.0 %copy-start.7 = (f32[1,2048]{1,0:T(1,128)S(1)}, f32[1,2048]{1,0:T(1,128)}, u32[]{:S(2)}) copy-start(f32[1,2048]{1,0:T(1,128)} %scale.17) | copy-start | bytes 24580
  78.4 12.4 %collective-permute-start.11 = (bf16[256,512]{1,0:T(8,128)(2,1)S(1)}, bf16[256,512]{1,0:T(8,128)(2,1)S(1)}, u32[]{:S(2)}, u32[]{:S(2)}) collective-permute-start(bf16[256,512]{1,0:T(8,128)(2,1)S(1)} %shard_map.94.refs_8_), channel_id=1, source_target_pairs={{0,1},{1,0},{2,3},{3,2},{4,5},{5,4},{6,7},{7,6},{8,9},{9,8},{10,11... | collective-permute-start | bytes 786440 | tf_op jit(solution)/shard_map/ppermute | solution.py:284
  78.6 12.8 %collective-permute-start.8 = (bf16[256,512]{1,0:T(8,128)(2,1)S(1)}, bf16[256,512]{1,0:T(8,128)(2,1)S(1)}, u32[]{:S(2)}, u32[]{:S(2)}) collective-permute-start(bf16[256,512]{1,0:T(8,128)(2,1)S(1)} %shard_map.93.refs_4_), channel_id=1, source_target_pairs={{0,2},{1,3},{2,0},{3,1},{4,6},{5,7},{6,4},{7,5},{8,10},{9,11},{10,... | collective-permute-start | bytes 786440 | tf_op jit(solution)/shard_map/ppermute | solution.py:284
  84.2 7.2 %collective-permute-start.7 = (bf16[256,512]{1,0:T(8,128)(2,1)S(1)}, bf16[256,512]{1,0:T(8,128)(2,1)S(1)}, u32[]{:S(2)}, u32[]{:S(2)}) collective-permute-start(bf16[256,512]{1,0:T(8,128)(2,1)S(1)} %shard_map.93.refs_4_), channel_id=1, source_target_pairs={{0,1},{1,0},{2,3},{3,2},{4,5},{5,4},{6,7},{7,6},{8,9},{9,8},{10,11... | collective-permute-start | bytes 786440 | tf_op jit(solution)/shard_map/ppermute | solution.py:284
  89.3 7.9 %collective-permute-start.16 = (bf16[256,512]{1,0:T(8,128)(2,1)S(1)}, bf16[256,512]{1,0:T(8,128)(2,1)S(1)}, u32[]{:S(2)}, u32[]{:S(2)}) collective-permute-start(bf16[256,512]{1,0:T(8,128)(2,1)S(1)} %shard_map.95.refs_12_), channel_id=1, source_target_pairs={{0,2},{1,3},{2,0},{3,1},{4,6},{5,7},{6,4},{7,5},{8,10},{9,11},{10,... | collective-permute-start | bytes 786440 | tf_op jit(solution)/shard_map/ppermute | solution.py:284
  90.8 6.4 %collective-permute-start.5 = (bf16[256,512]{1,0:T(8,128)(2,1)S(1)}, bf16[256,512]{1,0:T(8,128)(2,1)S(1)}, u32[]{:S(2)}, u32[]{:S(2)}) collective-permute-start(bf16[256,512]{1,0:T(8,128)(2,1)S(1)} %collective-permute-done.4.refs_2_), channel_id=1, source_target_pairs={{0,1},{1,0},{2,3},{3,2},{4,5},{5,4},{6,7},{7,6},{8,9},{9,8},{10,11... | collective-permute-start | bytes 786440 | tf_op jit(solution)/shard_map/ppermute | solution.py:284
  90.8 7.9 %collective-permute-start.13 = (bf16[256,512]{1,0:T(8,128)(2,1)S(1)}, bf16[256,512]{1,0:T(8,128)(2,1)S(1)}, u32[]{:S(2)}, u32[]{:S(2)}) collective-permute-start(bf16[256,512]{1,0:T(8,128)(2,1)S(1)} %collective-permute-done.12.refs_10_), channel_id=1, source_target_pairs={{0,1},{1,0},{2,3},{3,2},{4,5},{5,4},{6,7},{7,6},{8,9},{9,8},{10,11... | collective-permute-start | bytes 786440 | tf_op jit(solution)/shard_map/ppermute | solution.py:284
  91.3 7.9 %collective-permute-start.9 = (bf16[256,512]{1,0:T(8,128)(2,1)S(1)}, bf16[256,512]{1,0:T(8,128)(2,1)S(1)}, u32[]{:S(2)}, u32[]{:S(2)}) collective-permute-start(bf16[256,512]{1,0:T(8,128)(2,1)S(1)} %collective-permute-done.8.refs_6_), channel_id=1, source_target_pairs={{0,1},{1,0},{2,3},{3,2},{4,5},{5,4},{6,7},{7,6},{8,9},{9,8},{10,11... | collective-permute-start | bytes 786440 | tf_op jit(solution)/shard_map/ppermute | solution.py:284
  91.4 9.3 %collective-permute-start.15 = (bf16[256,512]{1,0:T(8,128)(2,1)S(1)}, bf16[256,512]{1,0:T(8,128)(2,1)S(1)}, u32[]{:S(2)}, u32[]{:S(2)}) collective-permute-start(bf16[256,512]{1,0:T(8,128)(2,1)S(1)} %shard_map.95.refs_12_), channel_id=1, source_target_pairs={{0,1},{1,0},{2,3},{3,2},{4,5},{5,4},{6,7},{7,6},{8,9},{9,8},{10,11... | collective-permute-start | bytes 786440 | tf_op jit(solution)/shard_map/ppermute | solution.py:284
  97.2 3.6 %collective-permute-start.17 = (bf16[256,512]{1,0:T(8,128)(2,1)S(1)}, bf16[256,512]{1,0:T(8,128)(2,1)S(1)}, u32[]{:S(2)}, u32[]{:S(2)}) collective-permute-start(bf16[256,512]{1,0:T(8,128)(2,1)S(1)} %collective-permute-done.16.refs_14_), channel_id=1, source_target_pairs={{0,1},{1,0},{2,3},{3,2},{4,5},{5,4},{6,7},{7,6},{8,9},{9,8},{10,11... | collective-permute-start | bytes 786440 | tf_op jit(solution)/shard_map/ppermute | solution.py:284
  97.2 9.2 %collective-permute-start.34 = (bf16[256,512]{1,0:T(8,128)(2,1)S(1)}, bf16[256,512]{1,0:T(8,128)(2,1)S(1)}, u32[]{:S(2)}, u32[]{:S(2)}) collective-permute-start(bf16[256,512]{1,0:T(8,128)(2,1)S(1)} %collective-permute-done.33.refs_0_), channel_id=1, source_target_pairs={{0,16},{1,17},{2,18},{3,19},{4,20},{5,21},{6,22},{7,23},{8,24},{9,... | collective-permute-start | bytes 786440 | tf_op jit(solution)/shard_map/ppermute | solution.py:284
  98.7 13.3 %collective-permute-start.27 = (bf16[256,512]{1,0:T(8,128)(2,1)S(1)}, bf16[256,512]{1,0:T(8,128)(2,1)S(1)}, u32[]{:S(2)}, u32[]{:S(2)}) collective-permute-start(bf16[256,512]{1,0:T(8,128)(2,1)S(1)} %collective-permute-done.26.refs_0_), channel_id=1, source_target_pairs={{0,16},{1,17},{2,18},{3,19},{4,20},{5,21},{6,22},{7,23},{8,24},{9,... | collective-permute-start | bytes 786440 | tf_op jit(solution)/shard_map/ppermute | solution.py:284
  99.2 17.9 %collective-permute-start.41 = (bf16[256,512]{1,0:T(8,128)(2,1)S(1)}, bf16[256,512]{1,0:T(8,128)(2,1)S(1)}, u32[]{:S(2)}, u32[]{:S(2)}) collective-permute-start(bf16[256,512]{1,0:T(8,128)(2,1)S(1)} %collective-permute-done.40.refs_0_), channel_id=1, source_target_pairs={{0,16},{1,17},{2,18},{3,19},{4,20},{5,21},{6,22},{7,23},{8,24},{9,... | collective-permute-start | bytes 786440 | tf_op jit(solution)/shard_map/ppermute | solution.py:284
  107.7 10.9 %collective-permute-start.35 = (bf16[512,512]{1,0:T(8,128)(2,1)S(1)}, bf16[512,512]{1,0:T(8,128)(2,1)S(1)}, u32[]{:S(2)}, u32[]{:S(2)}) collective-permute-start(bf16[512,512]{1,0:T(8,128)(2,1)S(1)} %get-tuple-element.61), channel_id=1, source_target_pairs={{0,1},{1,0},{2,3},{3,2},{4,5},{5,4},{6,7},{7,6},{8,9},{9,8},{10,11... | collective-permute-start | bytes 1572872 | tf_op jit(solution)/shard_map/ppermute | solution.py:284
  113.3 7.5 %collective-permute-start.28 = (bf16[512,512]{1,0:T(8,128)(2,1)S(1)}, bf16[512,512]{1,0:T(8,128)(2,1)S(1)}, u32[]{:S(2)}, u32[]{:S(2)}) collective-permute-start(bf16[512,512]{1,0:T(8,128)(2,1)S(1)} %get-tuple-element.52), channel_id=1, source_target_pairs={{0,1},{1,0},{2,3},{3,2},{4,5},{5,4},{6,7},{7,6},{8,9},{9,8},{10,11... | collective-permute-start | bytes 1572872 | tf_op jit(solution)/shard_map/ppermute | solution.py:284
  113.4 8.7 %collective-permute-start.24 = (bf16[512,512]{1,0:T(8,128)(2,1)S(1)}, bf16[512,512]{1,0:T(8,128)(2,1)S(1)}, u32[]{:S(2)}, u32[]{:S(2)}) collective-permute-start(bf16[512,512]{1,0:T(8,128)(2,1)S(1)} %get-tuple-element.47), channel_id=1, source_target_pairs={{0,1},{1,0},{2,3},{3,2},{4,5},{5,4},{6,7},{7,6},{8,9},{9,8},{10,11... | collective-permute-start | bytes 1572872 | tf_op jit(solution)/shard_map/ppermute | solution.py:284
  118.5 5.9 %collective-permute-start.42 = (bf16[512,512]{1,0:T(8,128)(2,1)S(1)}, bf16[512,512]{1,0:T(8,128)(2,1)S(1)}, u32[]{:S(2)}, u32[]{:S(2)}) collective-permute-start(bf16[512,512]{1,0:T(8,128)(2,1)S(1)} %get-tuple-element.70), channel_id=1, source_target_pairs={{0,1},{1,0},{2,3},{3,2},{4,5},{5,4},{6,7},{7,6},{8,9},{9,8},{10,11... | collective-permute-start | bytes 1572872 | tf_op jit(solution)/shard_map/ppermute | solution.py:284
  119.2 9.2 %collective-permute-start.36 = (bf16[256,512]{1,0:T(8,128)(2,1)S(1)}, bf16[256,512]{1,0:T(8,128)(2,1)S(1)}, u32[]{:S(2)}, u32[]{:S(2)}) collective-permute-start(bf16[256,512]{1,0:T(8,128)(2,1)S(1)} %get-tuple-element.63), channel_id=1, source_target_pairs={{0,2},{1,3},{2,0},{3,1},{4,6},{5,7},{6,4},{7,5},{8,10},{9,11},{10,... | collective-permute-start | bytes 786440 | tf_op jit(solution)/shard_map/ppermute | solution.py:284
  121.5 12.9 %collective-permute-start.29 = (bf16[256,512]{1,0:T(8,128)(2,1)S(1)}, bf16[256,512]{1,0:T(8,128)(2,1)S(1)}, u32[]{:S(2)}, u32[]{:S(2)}) collective-permute-start(bf16[256,512]{1,0:T(8,128)(2,1)S(1)} %get-tuple-element.54), channel_id=1, source_target_pairs={{0,2},{1,3},{2,0},{3,1},{4,6},{5,7},{6,4},{7,5},{8,10},{9,11},{10,... | collective-permute-start | bytes 786440 | tf_op jit(solution)/shard_map/ppermute | solution.py:284
  122.8 16.9 %collective-permute-start.25 = (bf16[256,512]{1,0:T(8,128)(2,1)S(1)}, bf16[256,512]{1,0:T(8,128)(2,1)S(1)}, u32[]{:S(2)}, u32[]{:S(2)}) collective-permute-start(bf16[256,512]{1,0:T(8,128)(2,1)S(1)} %get-tuple-element.49), channel_id=1, source_target_pairs={{0,2},{1,3},{2,0},{3,1},{4,6},{5,7},{6,4},{7,5},{8,10},{9,11},{10,... | collective-permute-start | bytes 786440 | tf_op jit(solution)/shard_map/ppermute | solution.py:284
  125.0 22.0 %collective-permute-start.43 = (bf16[256,512]{1,0:T(8,128)(2,1)S(1)}, bf16[256,512]{1,0:T(8,128)(2,1)S(1)}, u32[]{:S(2)}, u32[]{:S(2)}) collective-permute-start(bf16[256,512]{1,0:T(8,128)(2,1)S(1)} %get-tuple-element.72), channel_id=1, source_target_pairs={{0,2},{1,3},{2,0},{3,1},{4,6},{5,7},{6,4},{7,5},{8,10},{9,11},{10,... | collective-permute-start | bytes 786440 | tf_op jit(solution)/shard_map/ppermute | solution.py:284
  129.1 19.0 %collective-permute-start.37 = (bf16[64,512]{1,0:T(8,128)(2,1)S(1)}, bf16[64,512]{1,0:T(8,128)(2,1)S(1)}, u32[]{:S(2)}, u32[]{:S(2)}) collective-permute-start(bf16[64,512]{1,0:T(8,128)(2,1)S(1)} %get-tuple-element.65), channel_id=1, source_target_pairs={{0,4},{1,5},{2,6},{3,7},{4,0},{5,1},{6,2},{7,3},{8,12},{9,13},{10,... | collective-permute-start | bytes 196616 | tf_op jit(solution)/shard_map/ppermute | solution.py:284
  131.8 19.0 %collective-permute-start.38 = (bf16[64,512]{1,0:T(8,128)(2,1)S(1)}, bf16[64,512]{1,0:T(8,128)(2,1)S(1)}, u32[]{:S(2)}, u32[]{:S(2)}) collective-permute-start(bf16[64,512]{1,0:T(8,128)(2,1)S(1)} %get-tuple-element.66), channel_id=1, source_target_pairs={{0,8},{1,9},{2,10},{3,11},{4,12},{5,13},{6,14},{7,15},{8,0},{9,1},... | collective-permute-start | bytes 196616 | tf_op jit(solution)/shard_map/ppermute | solution.py:284
  140.4 27.0 %collective-permute-start.30 = (bf16[64,1024]{1,0:T(8,128)(2,1)S(1)}, bf16[64,1024]{1,0:T(8,128)(2,1)S(1)}, u32[]{:S(2)}, u32[]{:S(2)}) collective-permute-start(bf16[64,1024]{1,0:T(8,128)(2,1)S(1)} %get-tuple-element.56), channel_id=1, source_target_pairs={{0,4},{1,5},{2,6},{3,7},{4,0},{5,1},{6,2},{7,3},{8,12},{9,13},{10,... | collective-permute-start | bytes 393224 | tf_op jit(solution)/shard_map/ppermute | solution.py:284
  143.0 9.1 %collective-permute-start.39 = (bf16[64,512]{1,0:T(8,128)(2,1)S(1)}, bf16[64,512]{1,0:T(8,128)(2,1)S(1)}, u32[]{:S(2)}, u32[]{:S(2)}) collective-permute-start(bf16[64,512]{1,0:T(8,128)(2,1)S(1)} %get-tuple-element.67), channel_id=1, source_target_pairs={{0,12},{1,13},{2,14},{3,15},{4,8},{5,9},{6,10},{7,11},{8,4},{9,5},... | collective-permute-start | bytes 196616 | tf_op jit(solution)/shard_map/ppermute | solution.py:284
  147.6 6.5 %collective-permute-start.44 = (bf16[64,512]{1,0:T(8,128)(2,1)S(1)}, bf16[64,512]{1,0:T(8,128)(2,1)S(1)}, u32[]{:S(2)}, u32[]{:S(2)}) collective-permute-start(bf16[64,512]{1,0:T(8,128)(2,1)S(1)} %get-tuple-element.74), channel_id=1, source_target_pairs={{0,4},{1,5},{2,6},{3,7},{4,0},{5,1},{6,2},{7,3},{8,12},{9,13},{10,... | collective-permute-start | bytes 196616 | tf_op jit(solution)/shard_map/ppermute | solution.py:284
  148.1 19.3 %collective-permute-start.31 = (bf16[64,1024]{1,0:T(8,128)(2,1)S(1)}, bf16[64,1024]{1,0:T(8,128)(2,1)S(1)}, u32[]{:S(2)}, u32[]{:S(2)}) collective-permute-start(bf16[64,1024]{1,0:T(8,128)(2,1)S(1)} %get-tuple-element.57), channel_id=1, source_target_pairs={{0,8},{1,9},{2,10},{3,11},{4,12},{5,13},{6,14},{7,15},{8,0},{9,1},... | collective-permute-start | bytes 393224 | tf_op jit(solution)/shard_map/ppermute | solution.py:284
  150.7 16.7 %collective-permute-start.32 = (bf16[64,1024]{1,0:T(8,128)(2,1)S(1)}, bf16[64,1024]{1,0:T(8,128)(2,1)S(1)}, u32[]{:S(2)}, u32[]{:S(2)}) collective-permute-start(bf16[64,1024]{1,0:T(8,128)(2,1)S(1)} %get-tuple-element.58), channel_id=1, source_target_pairs={{0,12},{1,13},{2,14},{3,15},{4,8},{5,9},{6,10},{7,11},{8,4},{9,5},... | collective-permute-start | bytes 393224 | tf_op jit(solution)/shard_map/ppermute | solution.py:284
  152.2 15.2 %collective-permute-start.45 = (bf16[64,512]{1,0:T(8,128)(2,1)S(1)}, bf16[64,512]{1,0:T(8,128)(2,1)S(1)}, u32[]{:S(2)}, u32[]{:S(2)}) collective-permute-start(bf16[64,512]{1,0:T(8,128)(2,1)S(1)} %get-tuple-element.75), channel_id=1, source_target_pairs={{0,8},{1,9},{2,10},{3,11},{4,12},{5,13},{6,14},{7,15},{8,0},{9,1},... | collective-permute-start | bytes 196616 | tf_op jit(solution)/shard_map/ppermute | solution.py:284
  154.2 13.3 %collective-permute-start.46 = (bf16[64,512]{1,0:T(8,128)(2,1)S(1)}, bf16[64,512]{1,0:T(8,128)(2,1)S(1)}, u32[]{:S(2)}, u32[]{:S(2)}) collective-permute-start(bf16[64,512]{1,0:T(8,128)(2,1)S(1)} %get-tuple-element.76), channel_id=1, source_target_pairs={{0,12},{1,13},{2,14},{3,15},{4,8},{5,9},{6,10},{7,11},{8,4},{9,5},... | collective-permute-start | bytes 196616 | tf_op jit(solution)/shard_map/ppermute | solution.py:284
  168.2 6.4 %collective-permute-start.48 = (bf16[64,2048]{1,0:T(8,128)(2,1)S(1)}, bf16[64,2048]{1,0:T(8,128)(2,1)S(1)}, u32[]{:S(2)}, u32[]{:S(2)}) collective-permute-start(bf16[64,2048]{1,0:T(8,128)(2,1)S(1)} %shard_map.110.refs_0_), channel_id=1, source_target_pairs={{0,2},{1,3},{2,0},{3,1},{4,6},{5,7},{6,4},{7,5},{8,10},{9,11},{10,... | collective-permute-start | bytes 786440 | tf_op jit(solution)/shard_map/ppermute | solution.py:284
  169.9 4.7 %collective-permute-start.47 = (bf16[64,2048]{1,0:T(8,128)(2,1)S(1)}, bf16[64,2048]{1,0:T(8,128)(2,1)S(1)}, u32[]{:S(2)}, u32[]{:S(2)}) collective-permute-start(bf16[64,2048]{1,0:T(8,128)(2,1)S(1)} %shard_map.110.refs_0_), channel_id=1, source_target_pairs={{0,1},{1,0},{2,3},{3,2},{4,5},{5,4},{6,7},{7,6},{8,9},{9,8},{10,11... | collective-permute-start | bytes 786440 | tf_op jit(solution)/shard_map/ppermute | solution.py:284
  174.6 1.5 collective-permute-start.49
